TPU v7x, 256 devices: a whole 4x4x8 slice. The times are simulated.
256 devices in a mesh: sp: 16 (over y, x), dp: 16 (over z, core).
Axes of the slice: x: 4, y: 4, z: 8, core: 2. Of those that a mesh axis runs over, the one named last changes fastest.
Arguments:
- value_half: bfloat16 [16, 4096, 2048], P('dp', 'sp'), may hold values from -6 to 6
- gate_half: bfloat16 [16, 4096, 2048], P('dp', 'sp'), may hold values from -6 to 6
- upstream: bfloat16 [16, 4096, 2048], P('dp', 'sp'), may hold values from -6 to 6
- conv_taps: float32 [31, 2048], P(None, 'sp'), may hold values from -1 to 1
- norm_gain: float32 [2048], replicated, may hold values from 0.1 to 1.9
- out_weight: bfloat16 [2048, 2048], P('dp'), may hold values from -0.125 to 0.125
Outputs:
- grad_value: bfloat16 [16, 4096, 2048], P('dp', 'sp')
- grad_gate: bfloat16 [16, 4096, 2048], P('dp', 'sp')
- grad_taps: float32 [31, 2048], P(None, 'sp')
- grad_gain: float32 [2048], replicated
- grad_weight: float32 [2048, 2048], P('dp')
All inputs are finite; a program needn't handle non-finite values.
Results may differ from a plain program's by a relative error of at most 0.0062.
Values may be sent and summed in bfloat16 or wider, within the bound.
A program may use at most 128 MiB of HBM per device.

v0:
```python
import functools

import jax
import jax.numpy as jnp
from jax import lax
from jax.sharding import Mesh
from jax.sharding import PartitionSpec as P

DP = ("dp_0", "dp_1")
SP = ("sp_0", "sp_1")
SP_DP = ("sp_0", "sp_1", "dp_0", "dp_1")


NORM_EPS = 1e-05


def from_everyone(shard, axis):
    count = lax.axis_size(axis)
    return lax.all_to_all(
        jnp.broadcast_to(shard[None], (count, *shard.shape)), axis, 0, 0, tiled=True
    )


def of_everyone(shard, axis):
    return from_everyone(shard, axis).sum(axis=0)


def one_axis_at_a_time(shard, axes):
    return functools.reduce(lax.psum, axes, shard)


def body(value_half, gate_half, upstream, conv_taps, norm_gain, out_weight):
    tap_count = conv_taps.shape[0]
    sig_gate = jax.nn.sigmoid(gate_half.astype(jnp.float32))
    value_wide = value_half.astype(jnp.float32)
    glu = (value_wide * sig_gate).astype(jnp.bfloat16)
    glu_heads = lax.all_to_all(glu, SP, split_axis=2, concat_axis=1, tiled=True).astype(jnp.float32)
    length = glu_heads.shape[1]
    padded = jnp.pad(glu_heads, ((0, 0), (tap_count - 1, 0), (0, 0)))
    conv_out = jnp.zeros_like(glu_heads)
    for offset in range(tap_count):
        conv_out = conv_out + conv_taps[offset] * padded[:, offset : offset + length]
    conv_tokens = lax.all_to_all(
        conv_out.astype(jnp.bfloat16), SP, split_axis=1, concat_axis=2, tiled=True
    ).astype(jnp.float32)
    row_mean = jnp.mean(conv_tokens, axis=-1, keepdims=True)
    centered = conv_tokens - row_mean
    inv_scale = lax.rsqrt(jnp.mean(centered * centered, axis=-1, keepdims=True) + NORM_EPS)
    normed = centered * inv_scale
    scaled = normed * norm_gain
    sig_scaled = jax.nn.sigmoid(scaled)
    activated = (scaled * sig_scaled).astype(jnp.bfloat16)[0]
    upstream_rows = upstream[0]
    columns = upstream_rows
    grad_act = jnp.dot(
        columns,
        lax.all_gather(out_weight, DP, axis=0, tiled=True),
        preferred_element_type=jnp.float32,
    )
    grad_scaled = grad_act[None] * sig_scaled * (1.0 + scaled * (1.0 - sig_scaled))
    gain_part = jnp.sum(grad_scaled * normed, axis=(0, 1))
    grad_normed = grad_scaled * norm_gain
    grad_conv_out = inv_scale * (
        grad_normed
        - jnp.mean(grad_normed, axis=-1, keepdims=True)
        - normed * jnp.mean(grad_normed * normed, axis=-1, keepdims=True)
    )
    grad_heads = lax.all_to_all(
        grad_conv_out.astype(jnp.bfloat16), SP, split_axis=2, concat_axis=1, tiled=True
    ).astype(jnp.float32)
    grad_padded = jnp.pad(grad_heads, ((0, 0), (0, tap_count - 1), (0, 0)))
    grad_glu = jnp.zeros_like(grad_heads)
    tap_terms = []
    for offset in range(tap_count):
        first = tap_count - 1 - offset
        grad_glu = grad_glu + conv_taps[offset] * grad_padded[:, first : first + length]
        tap_terms.append(jnp.sum(grad_heads * padded[:, offset : offset + length], axis=(0, 1)))
    grad_taps = of_everyone(jnp.stack(tap_terms), DP)
    grad_tokens = lax.all_to_all(
        grad_glu.astype(jnp.bfloat16), SP, split_axis=1, concat_axis=2, tiled=True
    ).astype(jnp.float32)
    grad_value = (grad_tokens * sig_gate).astype(jnp.bfloat16)
    grad_gate = (grad_tokens * value_wide * sig_gate * (1.0 - sig_gate)).astype(jnp.bfloat16)
    grad_gain = one_axis_at_a_time(gain_part, SP_DP)
    columns = upstream_rows
    owned = lax.psum_scatter(
        lax.dot_general(
            columns, activated, (((0,), (0,)), ((), ())), preferred_element_type=jnp.float32
        ),
        DP,
        scatter_dimension=0,
        tiled=True,
    )
    grad_weight = lax.psum(owned, SP)
    return (grad_value, grad_gate, grad_taps, grad_gain, grad_weight)


def solution(mesh):
    torus = Mesh(mesh.devices.reshape(4, 4, 8, 2), ("sp_0", "sp_1", "dp_0", "dp_1"))
    placed = (P(DP, SP, None), P(DP, SP, None), P(DP, SP, None), P(None, SP), P(), P(DP, None))
    return jax.shard_map(
        body,
        mesh=torus,
        in_specs=placed,
        out_specs=(P(DP, SP, None), P(DP, SP, None), P(None, SP), P(), P(DP, None)),
        check_vma=False,
    )
```

profile of v0, /device:TPU:1, one launch (start us, length us, event | category | flops | bytes accessed | tf_op | source)
XLA Modules:
  0.0 445.3 jit_solution(18143520017637400832)
XLA Ops:
  9.4 1.9 copy.76
  11.9 12.9 %copy.120 = bf16[1,256,2048]{1,0,2:T(2,128)(2,1)} copy(bf16[1,256,2048]{1,2,0:T(8,128)(2,1)S(1)} %fusion.1) | data formatting | bytes 2097152 | tf_op jit(solution)/shard_map/convert_element_type | solution.py:36
  25.3 11.6 %reduce.17 = bf16[2048,256]{1,0:T(8,128)(2,1)S(1)} reduce(bf16[2048,1,256]{2,1,0:T(2,128)(2,1)} %bitcast.226, bf16[]{:T(256)} %broadcast.202), dimensions={1}, to_apply=%bitcast.207.reduce_sub_computation | reduce | bytes 2097154
  38.1 7.6 %all-to-all-start = ((bf16[16,2,16384]{2,1,0:T(2,128)(2,1)}), bf16[16,2,16384]{2,1,0:T(2,128)(2,1)}, u32[]{:S(2)}, u32[]{:S(2)}) async-start(bf16[16,2,16384]{2,1,0:T(2,128)(2,1)} %reshape.390), calls=%async_computation | async-start | bytes 2097152 | tf_op jit(solution)/shard_map/all_to_all | solution.py:37
  46.3 15.5 %all-to-all-done = bf16[16,2,16384]{2,1,0:T(2,128)(2,1)} async-done(((bf16[16,2,16384]{2,1,0:T(2,128)(2,1)}), bf16[16,2,16384]{2,1,0:T(2,128)(2,1)}, u32[]{:S(2)}, u32[]{:S(2)}) %all-to-all-start) | async-done | bytes 1048608 | tf_op jit(solution)/shard_map/all_to_all | solution.py:37
  61.8 4.3 reshape.391
  66.1 1.6 copy_convert_fusion.2
  68.1 1.9 copy.79
  70.0 8.6 %add_convert_fusion.1 = bf16[1,4096,128]{2,1,0:T(8,128)(2,1)S(1)} fusion(f32[128]{0:T(128)S(1)} %get-tuple-element.104, f32[128]{0:T(128)S(1)} %get-tuple-element.105, f32[128]{0:T(128)S(1)} %get-tuple-element.76, f32[128]{0:T(128)S(1)} %get-tuple-element.77, f32[128]{0:T(128)S(1)} %get-tuple-element.78, f32[128]{0:T(128)S(1)} %get-tuple-element.79, ...), kind=kLoop, calls=%fused_computation.83 | loop fusion | flops 32505856 | bytes 5258752 | tf_op jit(solution)/shard_map/convert_element_type | solution.py:44
  78.6 17.1 %copy.119 = bf16[1,4096,128]{2,0,1:T(2,128)(2,1)} copy(bf16[1,4096,128]{2,1,0:T(8,128)(2,1)S(1)} %add_convert_fusion.1) | data formatting | bytes 2097152 | tf_op jit(solution)/shard_map/convert_element_type | solution.py:44
  95.7 24.4 %reduce.18 = bf16[4096,128]{1,0:T(8,128)(2,1)} reduce(bf16[4096,1,128]{2,1,0:T(2,128)(2,1)} %bitcast.228, bf16[]{:T(256)} %broadcast.202), dimensions={1}, to_apply=%bitcast.206.reduce_sub_computation | reduce | bytes 2097154
  120.1 2.1 reshape.392
  122.2 19.5 %all_to_all.20 = bf16[16,2,16384]{2,1,0:T(2,128)(2,1)} all-to-all(bf16[16,2,16384]{2,1,0:T(2,128)(2,1)} %reshape.392), channel_id=1, replica_groups=mesh['sp_0'=4,'sp_1'=4,'dp_0'=8,'dp_1'=2] {'sp_0','sp_1'}, dimensions={0} | all-to-all | bytes 2097152 | tf_op jit(solution)/shard_map/all_to_all | solution.py:43
  141.7 5.8 %reshape.393 = bf16[4096,1,128]{2,1,0:T(2,128)(2,1)} reshape(bf16[16,2,16384]{2,1,0:T(2,128)(2,1)} %all_to_all.20) | data formatting | bytes 2097152
  147.5 2.2 fusion.33
  149.7 3.0 copy_convert_fusion.1
  152.7 2.9 copy.82
  155.7 2.0 fusion.11
  157.9 1.8 fusion.29
  159.7 2.3 copy.91
  162.0 9.3 %convolution_bitcast_fusion = f32[2048,2048]{0,1:T(8,128)} fusion(bf16[256,2048]{0,1:T(8,128)(2,1)} %bitcast.233, bf16[1,256,2048]{2,1,0:T(8,128)(2,1)S(1)} %copy-done), kind=kOutput, calls=%fused_computation | convolution fusion | flops 2147483648 | bytes 18874368 | tf_op jit(solution)/shard_map/dot_general | solution.py:87
  171.3 4.2 copy.83
  175.4 7.7 %multiply_reduce_fusion = (f32[2048]{0:T(1024)S(1)}, f32[256]{0:T(256)S(1)}, f32[256]{0:T(256)S(1)}, f32[256,2048]{1,0:T(8,128)S(1)}) fusion(f32[256]{0:T(256)S(1)} %add_rsqrt_fusion, f32[256]{0:T(256)S(1)} %broadcast_multiply_fusion.2, f32[32,8,16,128]{3,2,1,0:T(8,128)} %bitcast.224, f32[2048]{0:T(1024)S(1)} %copy-done.10, ...), kind=kOutput, calls=%fused_computation.22 | convolution fusion | flops 2156393984 | bytes 13651968 | tf_op jit(solution)/shard_map/dot_general | solution.py:55
  184.2 3.8 copy.84
  188.0 11.9 %reduce.19 = bf16[2048,256]{1,0:T(8,128)(2,1)S(1)} reduce(bf16[2048,1,256]{2,1,0:T(2,128)(2,1)} %bitcast.229, bf16[]{:T(256)} %broadcast.202), dimensions={1}, to_apply=%bitcast.194.reduce_sub_computation | reduce | bytes 2097154
  200.9 17.4 %all_to_all.42 = bf16[16,2,16384]{2,1,0:T(2,128)(2,1)S(1)} all-to-all(bf16[16,2,16384]{2,1,0:T(2,128)(2,1)} %reshape.394), channel_id=1, replica_groups=mesh['sp_0'=4,'sp_1'=4,'dp_0'=8,'dp_1'=2] {'sp_0','sp_1'}, dimensions={0} | all-to-all | bytes 2097152 | tf_op jit(solution)/shard_map/all_to_all | solution.py:68
  218.4 3.5 reshape.395
  221.8 3.1 copy_convert_fusion
  224.9 2.9 copy.86
  227.8 2.8 multiply_reduce_fusion.1
  231.6 2.5 multiply_reduce_fusion.2
  234.2 2.5 multiply_reduce_fusion.4
  236.7 2.5 multiply_reduce_fusion.3
  240.0 13.3 %all-to-all-start.4 = ((f32[16,31,128]{2,1,0:T(8,128)}), f32[16,31,128]{2,1,0:T(8,128)S(1)}, u32[]{:S(2)}, u32[]{:S(2)}) async-start(f32[16,31,128]{2,1,0:T(8,128)} %broadcast_in_dim.2), calls=%async_computation.4 | async-start | bytes 524288 | tf_op jit(solution)/shard_map/all_to_all | solution.py:19
  253.3 37.3 %add_convert_fusion = bf16[1,4096,128]{2,1,0:T(8,128)(2,1)S(1)} fusion(f32[1,4096,128]{2,1,0:T(8,128)} %bitcast.213, f32[128]{0:T(128)S(1)} %get-tuple-element.104, f32[128]{0:T(128)S(1)} %get-tuple-element.105, f32[128]{0:T(128)S(1)} %get-tuple-element.76, f32[128]{0:T(128)S(1)} %get-tuple-element.77, f32[128]{0:T(128)S(1)} %get-tuple-element.78, ...), kind=kLoop, calls=%fused_computation.54 | loop fusion | flops 32505856 | bytes 3161600 | tf_op jit(solution)/shard_map/convert_element_type | solution.py:80
  290.6 16.7 %copy.118 = bf16[1,4096,128]{2,0,1:T(2,128)(2,1)S(1)} copy(bf16[1,4096,128]{2,1,0:T(8,128)(2,1)S(1)} %add_convert_fusion) | data formatting | bytes 2097152 | tf_op jit(solution)/shard_map/convert_element_type | solution.py:80
  307.4 22.4 %reduce.20 = bf16[4096,128]{1,0:T(8,128)(2,1)S(1)} reduce(bf16[4096,1,128]{2,1,0:T(2,128)(2,1)S(1)} %bitcast.227, bf16[]{:T(256)} %broadcast.202), dimensions={1}, to_apply=%bitcast.205.reduce_sub_computation | reduce | bytes 2097154
  330.9 3.7 all-to-all-start.3
  335.3 14.0 %psum.35 = f32[2048]{0:T(1024)S(1)} all-reduce(f32[2048]{0:T(1024)S(1)} %get-tuple-element.40), channel_id=1, replica_groups=mesh['sp_0'=4,'sp_1'=4,'dp_0'=8,'dp_1'=2] {'sp_0'}, use_global_device_ids=true, to_apply=%region_39.40 | all-reduce | flops 2048 | bytes 16384 | tf_op jit(solution)/shard_map/psum | solution.py:29
  349.2 9.1 %psum.36 = f32[2048]{0:T(1024)S(1)} all-reduce(f32[2048]{0:T(1024)S(1)} %psum.35), channel_id=1, replica_groups=mesh['sp_0'=4,'sp_1'=4,'dp_0'=8,'dp_1'=2] {'sp_1'}, use_global_device_ids=true, to_apply=%region_40.41 | all-reduce | flops 2048 | bytes 16384 | tf_op jit(solution)/shard_map/psum | solution.py:29
  358.3 15.0 %psum.37 = f32[2048]{0:T(1024)S(1)} all-reduce(f32[2048]{0:T(1024)S(1)} %psum.36), channel_id=1, replica_groups=mesh['sp_0'=4,'sp_1'=4,'dp_0'=8,'dp_1'=2] {'dp_0'}, use_global_device_ids=true, to_apply=%region_41.42 | all-reduce | flops 2048 | bytes 16384 | tf_op jit(solution)/shard_map/psum | solution.py:29
  373.3 10.1 %psum.38 = f32[2048]{0:T(1024)} all-reduce(f32[2048]{0:T(1024)S(1)} %psum.37), channel_id=1, replica_groups=mesh['sp_0'=4,'sp_1'=4,'dp_0'=8,'dp_1'=2] {'dp_1'}, use_global_device_ids=true, to_apply=%region_42.43 | all-reduce | flops 2048 | bytes 16384 | tf_op jit(solution)/shard_map/psum | solution.py:29
  385.3 1.5 convert_bitcast_fusion
  386.8 3.1 copy.89
  389.9 3.4 fusion.4
  393.3 2.3 copy.93
  397.0 38.8 %all-reduce.4.cloned.1.call-done = f32[128,2048]{0,1:T(8,128)} async-done(((f32[128,2048]{0,1:T(8,128)}), f32[128,2048]{0,1:T(8,128)}) %all-reduce.4.cloned.1.call-update) | async-done | bytes 1048592 | tf_op jit(solution)/shard_map/psum | solution.py:94
  435.8 2.5 copy.94
  (56 shorter events, 14.6 us)
Async XLA Ops:
  7.2 154.8 %copy-start = (bf16[1,256,2048]{2,1,0:T(8,128)(2,1)S(1)}, bf16[1,256,2048]{2,1,0:T(8,128)(2,1)}, u32[]{:S(2)}) copy-start(bf16[1,256,2048]{2,1,0:T(8,128)(2,1)} %param.8) | copy-start | bytes 3145732
  7.2 168.3 %all-gather.2.cloned.1.call-start = ((), (), s32[]{:S(2)}) async-start(), calls=%async_computation.6 | async-start | bytes 8912896 | tf_op jit(solution)/shard_map/all_gather | solution.py:57
  9.4 2.5 copy-start.5
  11.3 13.5 %copy-start.7 = (bf16[1,256,2048]{1,2,0:T(8,128)(2,1)}, bf16[1,256,2048]{1,2,0:T(8,128)(2,1)S(1)}, u32[]{:S(2)}) copy-start(bf16[1,256,2048]{1,2,0:T(8,128)(2,1)S(1)} %copy.76) | copy-start | bytes 3145732
  37.0 9.3 %copy-start.11 = (f32[31,128]{1,0:T(8,128)S(1)}, f32[31,128]{1,0:T(8,128)}, u32[]{:S(2)}) copy-start(f32[31,128]{1,0:T(8,128)} %param.9) | copy-start | bytes 47620
  38.1 23.7 %all-to-all-start = ((bf16[16,2,16384]{2,1,0:T(2,128)(2,1)}), bf16[16,2,16384]{2,1,0:T(2,128)(2,1)}, u32[]{:S(2)}, u32[]{:S(2)}) async-start(bf16[16,2,16384]{2,1,0:T(2,128)(2,1)} %reshape.390), calls=%async_computation | async-start | bytes 2097152 | tf_op jit(solution)/shard_map/all_to_all | solution.py:37
  45.7 288.9 %reduce-scatter.2.cloned.1.call-start = ((), (), s32[]{:S(2)}) async-start(), calls=%async_computation.7 | async-start | bytes 17825792 | tf_op jit(solution)/shard_map/reduce_scatter | solution.py:86
  66.1 2.0 copy-start.4
  155.7 2.1 copy-start.10
  155.7 2.2 copy-start.3
  175.4 7.7 %copy-start.9 = (f32[1,256,16,128]{3,2,1,0:T(8,128)S(1)}, f32[1,256,16,128]{3,2,1,0:T(8,128)}, u32[]{:S(2)}) copy-start(f32[1,256,16,128]{3,2,1,0:T(8,128)} %copy.83) | copy-start | bytes 6291460
  227.8 3.0 copy-start.2
  240.0 90.8 %all-to-all-start.4 = ((f32[16,31,128]{2,1,0:T(8,128)}), f32[16,31,128]{2,1,0:T(8,128)S(1)}, u32[]{:S(2)}, u32[]{:S(2)}) async-start(f32[16,31,128]{2,1,0:T(8,128)} %broadcast_in_dim.2), calls=%async_computation.4 | async-start | bytes 524288 | tf_op jit(solution)/shard_map/all_to_all | solution.py:19
  330.9 53.2 %all-to-all-start.3 = ((bf16[16,2,16384]{2,1,0:T(2,128)(2,1)}), bf16[16,2,16384]{2,1,0:T(2,128)(2,1)S(1)}, u32[]{:S(2)}, u32[]{:S(2)}) async-start(bf16[16,2,16384]{2,1,0:T(2,128)(2,1)} %reshape.396), calls=%async_computation.3 | async-start | bytes 2097152 | tf_op jit(solution)/shard_map/all_to_all | solution.py:79
  334.5 101.2 %all-reduce.4.cloned.1.call-start = ((), (), s32[]{:S(2)}) async-start(), calls=%async_computation.8 | async-start | bytes 2097152 | tf_op jit(solution)/shard_map/psum | solution.py:94
  386.8 3.1 copy-start.6
  386.8 3.1 copy-start.8
  395.6 42.7 %copy-start.1 = (bf16[1,256,2048]{2,1,0:T(8,128)(2,1)S(1)}, bf16[1,256,2048]{2,1,0:T(8,128)(2,1)}, u32[]{:S(2)}) copy-start(bf16[1,256,2048]{2,1,0:T(8,128)(2,1)} %param.8) | copy-start | bytes 3145732
Sparse Core Ops, SparseCore 0:
  9.8 60.0 all-gather.1
  171.4 106.7 reduce-scatter.1
  338.6 97.1 all-reduce.3
where the time goes:
time: 452 us; the launch traced here: 445 us
  other arithmetic  148 us (33%)
  local copies, waits for them, and re-layouts  99.6 us (22%)
  blocking collectives  85.1 us (19%)
  waiting for transfers between devices  55.7 us (12%)
  starting transfers between devices  25.1 us (6%)
  matrix products  16.9 us (4%)
  between operations  14.5 us (3%)
    unnamed x4, other arithmetic  70.3 us
    psum x4, blocking collectives, one_axis_at_a_time(): return functools.reduce(lax.psum, axes, shard)  48.2 us
    psum x1, waiting for transfers between devices, body(): grad_weight = lax.psum(owned, SP)  38.8 us
    convert_element_type x1, other arithmetic, body(): grad_glu.astype(jnp.bfloat16)  37.3 us
    unnamed x38, local copies, waits for them, and re-layouts  30.8 us
    all_to_all x1, blocking collectives, body(): lax.all_to_all(conv_out.astype(jnp.bfloat16), SP, split_axis=1, concat_ax...  19.5 us
    all_to_all x1, blocking collectives, body(): lax.all_to_all(grad_conv_out.astype(jnp.bfloat16), SP, split_axis=2, conc...  17.4 us
    convert_element_type x1, local copies, waits for them, and re-layouts, body(): conv_out.astype(jnp.bfloat16)  17.1 us
  transfers between devices with their start and end apart: 6, of which 2 were waited for; matrix products, arithmetic and copies ran while one was open for 59% of the time, Pallas kernels for 0%

commit v1 on v0

v1 whole, which is shorter than its diff:
```python
import functools

import jax
import jax.numpy as jnp
from jax import lax
from jax.experimental import pallas as pl
from jax.experimental.pallas import tpu as pltpu
from jax.sharding import Mesh
from jax.sharding import PartitionSpec as P

DP = ("dp_0", "dp_1")
SP = ("sp_0", "sp_1")
NORM_EPS = 1e-05
MESH = pl.DeviceIdType.MESH
F32 = jnp.float32
BF16 = jnp.bfloat16

TOK = 256
CH = 2048
NC = CH // 128
TAPS = 31
NZ = 8
ORDER = (4, 3, 5, 2, 6, 1, 7, 0)
STAGES = ((0, 4), (4, 8))
N_SEND = 220


def kernel(
    v_hbm, g_hbm, u_hbm, w_hbm, taps_ref, gain_ref,
    gg_ref, gw_ref, dt_ref, dn_ref,
    v_s, g_s, u_s, usib, wbuf, tapsb, glu, conv, act, actsib, ut,
    pbuf, r1, r2, q, s1, s2, vz, rz, fg, gacc, gpad, mean_s, inv_s,
    halo_out, halo_in, ghalo_out, ghalo_in, dn, tg, tr, tz, tsib, tfin, gfull,
    local_sem, send_sem, recv_sem,
):
    cy, cx, cz, cc = (lax.axis_index(a) for a in ("sp_0", "sp_1", "dp_0", "dp_1"))
    sp = cy * 4 + cx
    other = 1 - cc
    sibling = {"dp_1": other}

    def zdev(d):
        return {"dp_0": lax.rem(cz + d + NZ, NZ)}

    def spdev(d):
        s = lax.rem(sp + d + 16, 16)
        return {"sp_0": s // 4, "sp_1": lax.rem(s, 4)}

    used = [0]
    started = []

    def send(src, dst, device):
        i = used[0]
        used[0] += 1
        copy = pltpu.make_async_remote_copy(
            src_ref=src, dst_ref=dst, send_sem=send_sem.at[i], recv_sem=recv_sem.at[i],
            device_id=device, device_id_type=MESH,
        )
        copy.start()
        started.append(copy)
        return copy

    loads = [
        pltpu.make_async_copy(w_hbm, wbuf.at[0, cc], local_sem.at[0]),
        pltpu.make_async_copy(v_hbm.at[0], v_s, local_sem.at[1]),
        pltpu.make_async_copy(g_hbm.at[0], g_s, local_sem.at[2]),
        pltpu.make_async_copy(u_hbm.at[0], u_s, local_sem.at[3]),
    ]
    for load in loads:
        load.start()

    barrier = pltpu.get_barrier_semaphore()
    pl.semaphore_signal(barrier, inc=1, device_id=sibling, device_id_type=MESH)
    for d in range(1, NZ):
        pl.semaphore_signal(barrier, inc=1, device_id=zdev(d), device_id_type=MESH)
    for d in range(1, 16):
        pl.semaphore_signal(barrier, inc=1, device_id=spdev(d), device_id_type=MESH)

    tapsb[sp, :TAPS] = taps_ref[...]
    tapsb[sp, TAPS:] = jnp.zeros((1, 128), F32)
    loads[0].wait()
    pl.semaphore_wait(barrier, 23)

    w_copies = {}

    def w_send(step, sub):
        rows = pl.ds(64 * sub, 64)
        lanes = (slice(0, 1024), slice(1024, 2048)) if step == 4 else (slice(None), slice(None))
        for way, sign in ((0, 1), (1, -1)):
            src = (-sign * (step - 1)) % NZ
            dst = (-sign * step) % NZ
            w_copies[step, sub, way] = send(
                wbuf.at[src, cc, rows, lanes[way]], wbuf.at[dst, cc, rows, lanes[way]], zdev(sign)
            )

    w_pair = {}

    def w_share(rel, sub):
        rows = pl.ds(64 * sub, 64)
        w_pair[rel, sub] = send(wbuf.at[rel, cc, rows], wbuf.at[rel, cc, rows], sibling)

    def w_event(step, sub):
        for way in (0, 1):
            w_copies[step, sub, way].wait_recv()
        if step < 4:
            w_send(step + 1, sub)
        for rel in sorted({step, (-step) % NZ}):
            w_share(rel, sub)

    w_send(1, 0)
    w_send(1, 1)
    taps_copies = [send(tapsb.at[sp], tapsb.at[sp], spdev(d)) for d in range(1, 16)]
    for load in loads[1:]:
        load.wait()
    u_copy = send(u_s, usib, sibling)
    w_share(0, 0)
    w_share(0, 1)

    def glu_rows(r):
        rows = pl.ds(r, 32)
        for c in range(NC):
            lanes = slice(128 * c, 128 * c + 128)
            wide = v_s[rows, lanes].astype(F32) * jax.nn.sigmoid(g_s[rows, lanes].astype(F32))
            narrow = wide.astype(BF16)
            glu[c, pl.ds(r + 32, 32), :] = narrow.astype(F32)
            yield lanes, narrow

    for lanes, narrow in glu_rows(TOK - 32):
        halo_out[:, lanes] = narrow
    halo_copy = send(halo_out, halo_in, spdev(1))

    def glu_step(i, carry):
        for _ in glu_rows(pl.multiple_of(i * 32, 32)):
            pass
        return carry

    lax.fori_loop(0, TOK // 32 - 1, glu_step, 0)

    u_copy.wait_recv()

    def transpose_step(k, carry):
        zb = lax.rem(cz + k, NZ)
        cols = pl.ds(pl.multiple_of(zb * 256 + cc * 128, 128), 128)
        ut[k, :, 0:256] = u_s[:, cols].T
        ut[k, :, 256:512] = usib[:, cols].T
        return carry

    lax.fori_loop(0, NZ, transpose_step, 0)

    for copy in taps_copies:
        copy.wait_recv()
    halo_copy.wait_recv()
    keep = (sp > 0).astype(F32)
    for c in range(NC):
        glu[c, 0:32, :] = halo_in[:, 128 * c : 128 * c + 128].astype(F32) * keep

    mean_s[...] = jnp.zeros_like(mean_s)

    def conv_chunk(c, carry):
        taps = [jnp.broadcast_to(tapsb[c, j : j + 1, :], (8, 128)) for j in range(TAPS)]

        def rows_step(i, carry):
            for k in range(4):
                r = pl.multiple_of(i * 32, 32) + 8 * k
                parts = [None] * 4
                for j in range(TAPS):
                    term = taps[j] * glu[c, pl.ds(r + 2 + j, 8), :]
                    parts[j % 4] = term if parts[j % 4] is None else parts[j % 4] + term
                total = (parts[0] + parts[1]) + (parts[2] + parts[3])
                total = total.astype(BF16).astype(F32)
                conv[c, pl.ds(r, 8), :] = total
                mean_s[pl.ds(r, 8), :] += total
            return carry

        return lax.fori_loop(0, TOK // 32, rows_step, carry)

    lax.fori_loop(0, 8, conv_chunk, 0)
    w_event(1, 0)
    lax.fori_loop(8, NC, conv_chunk, 0)

    def norm_step(i, carry):
        rows = pl.ds(pl.multiple_of(i * 32, 32), 32)
        mu = jnp.broadcast_to(jnp.sum(mean_s[rows, :], axis=1, keepdims=True) * (1.0 / CH), (32, 128))
        squares = jnp.zeros((32, 128), F32)
        for c in range(NC):
            centered = conv[c, rows, :] - mu
            squares = squares + centered * centered
        inv = lax.rsqrt(jnp.sum(squares, axis=1, keepdims=True) * (1.0 / CH) + NORM_EPS)
        inv = jnp.broadcast_to(inv, (32, 128))
        mean_s[rows, :] = mu
        inv_s[rows, :] = inv
        for c in range(NC):
            lanes = slice(128 * c, 128 * c + 128)
            scaled = (conv[c, rows, :] - mu) * inv * gain_ref[:, lanes]
            act[rows, lanes] = (scaled * jax.nn.sigmoid(scaled)).astype(BF16)
        return carry

    lax.fori_loop(0, 4, norm_step, 0)
    act_copies = [send(act.at[0:128], actsib.at[0:128], sibling)]
    lax.fori_loop(4, 8, norm_step, 0)
    act_copies.append(send(act.at[128:256], actsib.at[128:256], sibling))
    w_event(1, 1)
    for copy in act_copies:
        copy.wait_recv()

    axes = ((("sp_1", cx), ("sp_0", cy)), (("sp_0", cy), ("sp_1", cx)))

    def near(axis, d):
        name, at = axis
        return {name: lax.rem(at + d + 4, 4)}

    def part(axis, d):
        return lax.rem(axis[1] + d + 4, 4)

    def partial_sums(stage):
        for k in range(*STAGES[stage]):
            lhs = ut[ORDER[k]]
            for n in range(4):
                lanes = slice(512 * n, 512 * n + 512)
                total = jnp.dot(lhs[:, 0:256], act[:, lanes], preferred_element_type=F32)
                total = total + jnp.dot(lhs[:, 256:512], actsib[:, lanes], preferred_element_type=F32)
                narrow = total.astype(BF16)
                for h in range(2):
                    for p in range(4):
                        first = 64 * h + 16 * p
                        pbuf[h, p, k, :, lanes] = narrow[first : first + 16, :]

    rs_copies = {}

    def rs1_send(stage):
        zs = pl.ds(STAGES[stage][0], STAGES[stage][1] - STAGES[stage][0])
        for h in range(2):
            axis = axes[h][0]
            far = part(axis, 2)
            for way, sign, lanes in ((0, 1, slice(0, 1024)), (1, -1, slice(1024, 2048))):
                rs_copies[1, stage, h, way] = send(
                    pbuf.at[h, far, zs, :, lanes], r1.at[h, way, zs], near(axis, sign)
                )

    def rs1_mid(stage):
        zs = pl.ds(STAGES[stage][0], STAGES[stage][1] - STAGES[stage][0])
        for h in range(2):
            axis = axes[h][0]
            for way, sign, lanes in ((0, 1, slice(0, 1024)), (1, -1, slice(1024, 2048))):
                rs_copies[1, stage, h, way].wait_recv()
                to = part(axis, sign)

                def add(k, carry, h=h, to=to, way=way, lanes=lanes):
                    pbuf[h, to, k, :, lanes] = (
                        pbuf[h, to, k, :, lanes].astype(F32) + r1[h, way, k].astype(F32)
                    ).astype(BF16)
                    return carry

                lax.fori_loop(*STAGES[stage], add, 0)
                rs_copies[2, stage, h, way] = send(pbuf.at[h, to, zs], r2.at[h, way, zs], near(axis, sign))

    def rs1_fin(stage):
        zs = pl.ds(STAGES[stage][0], STAGES[stage][1] - STAGES[stage][0])
        for h in range(2):
            mine = part(axes[h][0], 0)
            axis = axes[h][1]
            for way in (0, 1):
                rs_copies[2, stage, h, way].wait_recv()

            def add(k, carry, h=h, mine=mine):
                for p in range(4):
                    lanes = slice(512 * p, 512 * p + 512)
                    q[h, p, k] = (
                        pbuf[h, mine, k, :, lanes].astype(F32)
                        + r2[h, 0, k, :, lanes].astype(F32)
                        + r2[h, 1, k, :, lanes].astype(F32)
                    ).astype(BF16)
                return carry

            lax.fori_loop(*STAGES[stage], add, 0)
            far = part(axis, 2)
            for way, sign, lanes in ((0, 1, slice(0, 256)), (1, -1, slice(256, 512))):
                rs_copies[3, stage, h, way] = send(
                    q.at[h, far, zs, :, lanes], s1.at[h, way, zs], near(axis, sign)
                )

    def rs2_mid(stage):
        zs = pl.ds(STAGES[stage][0], STAGES[stage][1] - STAGES[stage][0])
        for h in range(2):
            axis = axes[h][1]
            for way, sign, lanes in ((0, 1, slice(0, 256)), (1, -1, slice(256, 512))):
                rs_copies[3, stage, h, way].wait_recv()
                to = part(axis, sign)
                for k in range(*STAGES[stage]):
                    q[h, to, k, :, lanes] = (
                        q[h, to, k, :, lanes].astype(F32) + s1[h, way, k].astype(F32)
                    ).astype(BF16)
                rs_copies[4, stage, h, way] = send(q.at[h, to, zs], s2.at[h, way, zs], near(axis, sign))

    z_copies = {}

    def rs2_fin(stage):
        for h in range(2):
            mine = part(axes[h][1], 0)
            for way in (0, 1):
                rs_copies[4, stage, h, way].wait_recv()
            for k in range(*STAGES[stage]):
                vz[k, h] = (
                    q[h, mine, k].astype(F32) + s2[h, 0, k].astype(F32) + s2[h, 1, k].astype(F32)
                ).astype(BF16)
        for k in range(*STAGES[stage]):
            if ORDER[k]:
                z_copies[k] = send(vz.at[k], rz.at[k], zdev(ORDER[k]))

    gather_copies = []

    def rs3():
        total = vz[ORDER.index(0)].astype(F32)
        for k in range(NZ):
            if ORDER[k]:
                z_copies[k].wait_recv()
                total = total + rz[k].astype(F32)
        fg[sp] = total.astype(BF16)
        for d in range(1, 16):
            gather_copies.append(send(fg.at[sp], fg.at[sp], spdev(d)))

    def grad_block(rels, first=False):
        for rel in rels:
            for sub in (0, 1):
                w_pair[rel, sub].wait_recv()
        lhs = []
        for rel in rels:
            zb = lax.rem(cz + rel, NZ)
            lhs.append(u_s[:, pl.ds(pl.multiple_of(zb * 256, 256), 256)])

        def step(n, carry):
            lanes = pl.ds(pl.multiple_of(n * 512, 512), 512)
            total = None
            for left, rel in zip(lhs, rels):
                right = wbuf[rel, :, :, lanes].reshape(256, 512)
                term = jnp.dot(left, right, preferred_element_type=F32)
                total = term if total is None else total + term
            if first:
                gacc[:, lanes] = total
            else:
                gacc[:, lanes] += total
            return carry

        lax.fori_loop(0, 4, step, 0)

    partial_sums(0)
    rs1_send(0)
    partial_sums(1)
    rs1_send(1)
    w_event(2, 0)
    rs1_mid(0)
    grad_block((0, 1, 7), first=True)
    rs1_mid(1)
    w_event(2, 1)
    rs1_fin(0)
    w_event(3, 0)
    rs2_mid(0)
    rs1_fin(1)
    grad_block((2, 6))
    rs2_fin(0)
    w_event(3, 1)
    rs2_mid(1)
    grad_block((3, 5))
    w_event(4, 0)
    rs2_fin(1)
    w_event(4, 1)
    grad_block((4,))

    dn[...] = jnp.zeros_like(dn)

    def back_rows(r):
        rows = pl.ds(r, 32)
        mu = mean_s[rows, :]
        inv = inv_s[rows, :]
        sum1 = jnp.zeros((32, 128), F32)
        sum2 = jnp.zeros((32, 128), F32)
        for c in range(NC):
            lanes = slice(128 * c, 128 * c + 128)
            gain = gain_ref[:, lanes]
            normed = (conv[c, rows, :] - mu) * inv
            scaled = normed * gain
            sig = jax.nn.sigmoid(scaled)
            grad_scaled = gacc[rows, lanes] * sig * (1.0 + scaled * (1.0 - sig))
            gain_term = grad_scaled * normed
            dn[c] += (gain_term[0:8] + gain_term[8:16]) + (gain_term[16:24] + gain_term[24:32])
            grad_normed = grad_scaled * gain
            gacc[rows, lanes] = grad_normed
            sum1 = sum1 + grad_normed
            sum2 = sum2 + grad_normed * normed
        m1 = jnp.broadcast_to(jnp.sum(sum1, axis=1, keepdims=True) * (1.0 / CH), (32, 128))
        m2 = jnp.broadcast_to(jnp.sum(sum2, axis=1, keepdims=True) * (1.0 / CH), (32, 128))
        for c in range(NC):
            lanes = slice(128 * c, 128 * c + 128)
            normed = (conv[c, rows, :] - mu) * inv
            narrow = (inv * (gacc[rows, lanes] - m1 - normed * m2)).astype(BF16)
            gpad[c, rows, :] = narrow.astype(F32)
            yield lanes, narrow

    for lanes, narrow in back_rows(0):
        ghalo_out[:, lanes] = narrow
    ghalo_copy = send(ghalo_out, ghalo_in, spdev(-1))

    def back_step(i, carry):
        for _ in back_rows(pl.multiple_of(i * 32, 32)):
            pass
        return carry

    lax.fori_loop(1, TOK // 32, back_step, 0)

    def taps_chunk(c, carry):
        def rows_step(i, sums):
            r = pl.multiple_of(i * 8, 8)
            g = gpad[c, pl.ds(r, 8), :]
            return tuple(sums[j] + g * glu[c, pl.ds(r + 2 + j, 8), :] for j in range(TAPS))

        sums = lax.fori_loop(0, TOK // 8, rows_step, tuple(jnp.zeros((8, 128), F32) for _ in range(TAPS)))
        for j in range(TAPS):
            tg[c, j : j + 1, :] = jnp.sum(sums[j], axis=0, keepdims=True)
        tg[c, TAPS:, :] = jnp.sum(dn[c], axis=0, keepdims=True)
        return carry

    lax.fori_loop(0, NC, taps_chunk, 0)
    part_copies = [send(tg.at[lax.rem(sp + d, 16)], tr.at[d], spdev(d)) for d in range(1, 16)]

    rs3()

    ghalo_copy.wait_recv()
    keep_g = (sp < 15).astype(F32)
    for c in range(NC):
        gpad[c, TOK:, :] = ghalo_in[:, 128 * c : 128 * c + 128].astype(F32) * keep_g

    def grad_chunk(c, carry):
        taps = [jnp.broadcast_to(tapsb[c, j : j + 1, :], (8, 128)) for j in range(TAPS)]
        lanes = pl.ds(pl.multiple_of(c * 128, 128), 128)

        def rows_step(i, carry):
            base = pl.multiple_of(i * 32, 32)
            tiles = []
            for k in range(4):
                r = base + 8 * k
                parts = [None] * 4
                for j in range(TAPS):
                    term = taps[j] * gpad[c, pl.ds(r + 30 - j, 8), :]
                    parts[j % 4] = term if parts[j % 4] is None else parts[j % 4] + term
                tiles.append((parts[0] + parts[1]) + (parts[2] + parts[3]))
            gg_ref[pl.ds(base, 32), lanes] = jnp.concatenate(tiles, axis=0).astype(BF16)
            return carry

        return lax.fori_loop(0, TOK // 32, rows_step, carry)

    lax.fori_loop(0, 8, grad_chunk, 0)

    total = tg[sp]
    for d in range(1, 16):
        part_copies[d - 1].wait_recv()
        total = total + tr[d]
    tz[cz] = total
    tz_copies = [send(tz.at[cz], tz.at[cz], zdev(d)) for d in range(1, NZ)]

    lax.fori_loop(8, NC, grad_chunk, 0)

    for copy in tz_copies:
        copy.wait_recv()
    total = tz[0]
    for k in range(1, NZ):
        total = total + tz[k]
    tfin[...] = total
    pair_copy = send(tfin, tsib, sibling)
    pair_copy.wait_recv()
    total = tfin[...] + tsib[...]
    dt_ref[...] = total
    gfull[sp] = jnp.broadcast_to(total[TAPS:, :], (8, 128))
    gain_copies = [send(gfull.at[sp], gfull.at[sp], spdev(d)) for d in range(1, 16)]

    for copy in gather_copies:
        copy.wait_recv()
    for s in range(16):
        y, x = divmod(s, 4)
        gw_ref[16 * x : 16 * x + 16, 512 * y : 512 * y + 512] = fg[s, 0]
        gw_ref[64 + 16 * y : 80 + 16 * y, 512 * x : 512 * x + 512] = fg[s, 1]
    for copy in gain_copies:
        copy.wait_recv()
    dn_ref[...] = gfull[...]
    for copy in started:
        copy.wait_send()


def body(value_half, gate_half, upstream, conv_taps, norm_gain, out_weight):
    vmem = pl.BlockSpec(memory_space=pltpu.VMEM)
    hbm = pl.BlockSpec(memory_space=pl.ANY)
    grad_glu, grad_rows, taps, gain = pl.pallas_call(
        kernel,
        out_shape=(
            jax.ShapeDtypeStruct((TOK, CH), BF16),
            jax.ShapeDtypeStruct((128, CH), BF16),
            jax.ShapeDtypeStruct((32, 128), F32),
            jax.ShapeDtypeStruct((16, 8, 128), F32),
        ),
        in_specs=[hbm] * 4 + [vmem] * 2,
        out_specs=[vmem] * 4,
        scratch_shapes=[
            pltpu.VMEM((TOK, CH), BF16),
            pltpu.VMEM((TOK, CH), BF16),
            pltpu.VMEM((TOK, CH), BF16),
            pltpu.VMEM((TOK, CH), BF16),
            pltpu.VMEM((NZ, 2, 128, CH), BF16),
            pltpu.VMEM((NC, 32, 128), F32),
            pltpu.VMEM((NC, TOK + 32, 128), F32),
            pltpu.VMEM((NC, TOK, 128), F32),
            pltpu.VMEM((TOK, CH), BF16),
            pltpu.VMEM((TOK, CH), BF16),
            pltpu.VMEM((NZ, 128, 512), BF16),
            pltpu.VMEM((2, 4, NZ, 16, CH), BF16),
            pltpu.VMEM((2, 2, NZ, 16, 1024), BF16),
            pltpu.VMEM((2, 2, NZ, 16, 2048), BF16),
            pltpu.VMEM((2, 4, NZ, 16, 512), BF16),
            pltpu.VMEM((2, 2, NZ, 16, 256), BF16),
            pltpu.VMEM((2, 2, NZ, 16, 512), BF16),
            pltpu.VMEM((NZ, 2, 16, 512), BF16),
            pltpu.VMEM((NZ, 2, 16, 512), BF16),
            pltpu.VMEM((16, 2, 16, 512), BF16),
            pltpu.VMEM((TOK, CH), F32),
            pltpu.VMEM((NC, TOK + 32, 128), F32),
            pltpu.VMEM((TOK, 128), F32),
            pltpu.VMEM((TOK, 128), F32),
            pltpu.VMEM((32, CH), BF16),
            pltpu.VMEM((32, CH), BF16),
            pltpu.VMEM((32, CH), BF16),
            pltpu.VMEM((32, CH), BF16),
            pltpu.VMEM((NC, 8, 128), F32),
            pltpu.VMEM((NC, 32, 128), F32),
            pltpu.VMEM((16, 32, 128), F32),
            pltpu.VMEM((NZ, 32, 128), F32),
            pltpu.VMEM((32, 128), F32),
            pltpu.VMEM((32, 128), F32),
            pltpu.VMEM((16, 8, 128), F32),
            pltpu.SemaphoreType.DMA((4,)),
            pltpu.SemaphoreType.DMA((N_SEND,)),
            pltpu.SemaphoreType.DMA((N_SEND,)),
        ],
        compiler_params=pltpu.CompilerParams(
            collective_id=0, has_side_effects=True, vmem_limit_bytes=66_000_000
        ),
    )(value_half, gate_half, upstream, out_weight, conv_taps, norm_gain[None])
    sig_gate = jax.nn.sigmoid(gate_half.astype(F32))
    wide = grad_glu.astype(F32)[None]
    grad_value = (wide * sig_gate).astype(BF16)
    grad_gate = (wide * value_half.astype(F32) * sig_gate * (1.0 - sig_gate)).astype(BF16)
    return grad_value, grad_gate, taps[:TAPS], gain[:, 0, :].reshape(CH), grad_rows.astype(F32)


def solution(mesh):
    torus = Mesh(mesh.devices.reshape(4, 4, 8, 2), ("sp_0", "sp_1", "dp_0", "dp_1"))
    placed = (P(DP, SP, None), P(DP, SP, None), P(DP, SP, None), P(None, SP), P(), P(DP, None))
    return jax.shard_map(
        body,
        mesh=torus,
        in_specs=placed,
        out_specs=(P(DP, SP, None), P(DP, SP, None), P(None, SP), P(), P(DP, None)),
        check_vma=False,
    )
```

time: 452 us -> 111 us (0.25); the launches traced: 445 us -> 111 us
  other arithmetic: 148 us -> 5.36 us
  Pallas kernels: 0 us -> 103 us
  local copies, waits for them, and re-layouts: 99.6 us -> 2.05 us
  blocking collectives: 85.1 us -> 0 us
  waiting for transfers between devices: 55.7 us -> 0 us
  starting transfers between devices: 25.1 us -> 0 us
  matrix products: 16.9 us -> 0 us
  between operations: 14.5 us -> 0.65 us
    pallas_call x0 -> x1, Pallas kernels: none -> 103 us  [body(): pl.pallas_call(kernel, out_shape=(jax.ShapeDtypeStruct((TOK, CH), BF16),...]
    unnamed x4 -> x0, other arithmetic: 70.3 us -> none
    convert_element_type x10 -> x0, local copies, waits for them, and re-layouts: 67.8 us -> none  [the longest x1 17.1 us: body(): conv_out.astype(jnp.bfloat16)]
    convert_element_type x10 -> x2, other arithmetic: 61.9 us -> 5.36 us  [the longest x1 4.29 us: body(): (wide * value_half.astype(F32) * sig_gate * (1.0 - sig_gate)).astype(BF16)]
    psum x4 -> x0, blocking collectives: 48.2 us -> none  [one_axis_at_a_time(): return functools.reduce(lax.psum, axes, shard)]
    psum x1 -> x0, waiting for transfers between devices: 38.8 us -> none  [body(): grad_weight = lax.psum(owned, SP)]
    all_to_all x2 -> x0, blocking collectives: 36.9 us -> none  [the longest x1 19.5 us: body(): lax.all_to_all(conv_out.astype(jnp.bfloat16), SP, split_axis=1, concat_ax...]
    unnamed x38 -> x5, local copies, waits for them, and re-layouts: 30.8 us -> 0.61 us
  transfers between devices with their start and end apart: 6 -> 0, of which waited for: 2 -> 0; matrix products, arithmetic and copies ran while one was open for 59% -> 0% of each run, Pallas kernels for 0% -> 0%
where the time goes in v1:
time: 111 us
  Pallas kernels  103 us (93%)
  other arithmetic  5.36 us (5%)
  local copies, waits for them, and re-layouts  2.05 us (2%)
    pallas_call x1, Pallas kernels, body(): pl.pallas_call(kernel, out_shape=(jax.ShapeDtypeStruct((TOK, CH), BF16),...  103 us
    convert_element_type x1, other arithmetic, body(): (wide * value_half.astype(F32) * sig_gate * (1.0 - sig_gate)).astype(BF16)  4.29 us

profile of v1, /device:TPU:1, one launch (start us, length us, event | category | flops | bytes accessed | tf_op | source)
XLA Modules:
  0.0 111.0 jit_solution(3514042504630339724)
XLA Ops:
  0.6 103.0 %shard_map.101 = (bf16[256,2048]{1,0:T(8,128)(2,1)}, bf16[128,2048]{1,0:T(8,128)(2,1)}, f32[32,128]{1,0:T(8,128)}, f32[16,8,128]{2,1,0:T(8,128)}) custom-call(bf16[1,256,2048]{2,1,0:T(8,128)(2,1)} %v_hbm.1, bf16[1,256,2048]{2,1,0:T(8,128)(2,1)} %g_hbm.1, bf16[1,256,2048]{2,1,0:T(8,128)(2,1)} %u_hbm.1, bf16[128,2048]{1,0:T(8,128)(2,1)} %w_hbm.1, ...), custom_call_target="tpu_custom_call" | custom-call | tf_op jit(solution)/shard_map/pallas_call | solution.py:490
  103.6 0.0 copy-start
  103.6 4.3 %fusion.3 = (bf16[1,256,2048]{2,1,0:T(8,128)(2,1)}, bf16[1,256,2048]{2,1,0:T(8,128)(2,1)}) fusion(bf16[1,256,2048]{2,1,0:T(8,128)(2,1)} %v_hbm.1, bf16[256,2048]{1,0:T(8,128)(2,1)} %get-tuple-element.9, bf16[1,256,2048]{2,1,0:T(8,128)(2,1)} %g_hbm.1), kind=kLoop, calls=%fused_computation.5 | loop fusion | flops 6815744 | bytes 5242880 | tf_op jit(solution)/shard_map/convert_element_type | solution.py:547
  107.9 0.0 copy-start.1
  107.9 0.0 copy-done
  107.9 1.1 convert_element_type.20
  109.0 1.4 %slice.7 = f32[16,1,128]{2,1,0:T(1,128)} slice(f32[16,8,128]{2,1,0:T(8,128)} %get-tuple-element.11), slice={[0:16], [0:1], [0:128]} | slice | bytes 16384 | tf_op jit(solution)/shard_map/slice | solution.py:548
  110.4 0.0 copy-done.1
  110.4 0.6 copy.12
Async XLA Ops:
  103.6 4.3 %copy-start = (bf16[128,2048]{1,0:T(8,128)(2,1)S(1)}, bf16[128,2048]{1,0:T(8,128)(2,1)}, u32[]{:S(2)}) copy-start(bf16[128,2048]{1,0:T(8,128)(2,1)} %get-tuple-element.12) | copy-start | bytes 1572868
  107.9 2.5 %copy-start.1 = (f32[32,128]{1,0:T(8,128)S(1)}, f32[32,128]{1,0:T(8,128)}, u32[]{:S(2)}) copy-start(f32[32,128]{1,0:T(8,128)} %get-tuple-element.10) | copy-start | bytes 49156

commit v2 on v1

v2 whole, which is shorter than its diff:
```python
import functools

import jax
import jax.numpy as jnp
from jax import lax
from jax.experimental import pallas as pl
from jax.experimental.pallas import tpu as pltpu
from jax.sharding import Mesh
from jax.sharding import PartitionSpec as P

DP = ("dp_0", "dp_1")
SP = ("sp_0", "sp_1")
NORM_EPS = 1e-05
MESH = pl.DeviceIdType.MESH
F32 = jnp.float32
BF16 = jnp.bfloat16

TOK = 256
CH = 2048
NC = CH // 128
TAPS = 31
NZ = 8
N_SEND = 220


def kernel(
    v_hbm, g_hbm, u_hbm, w_hbm, taps_ref, gain_ref,
    gv_hbm, gt_hbm, gw_ref, dt_ref, dn_ref,
    v_s, g_s, u_s, usib, wbuf, tapsb, glu, conv, act, actsib, ut,
    pbuf, r1, r2, q, s1, s2, vz, rz, fg, gacc, gpad, mean_s, inv_s, gate_a, gate_b, gv_s, gt_s,
    halo_out, halo_in, ghalo_out, ghalo_in, dn, tg, tr, tz, tsib, tfin, gfull,
    local_sem, send_sem, recv_sem,
):
    cy, cx, cz, cc = (lax.axis_index(a) for a in ("sp_0", "sp_1", "dp_0", "dp_1"))
    sp = cy * 4 + cx
    other = 1 - cc
    sibling = {"dp_1": other}

    def zdev(d):
        return {"dp_0": lax.rem(cz + d + NZ, NZ)}

    def spdev(d):
        s = lax.rem(sp + d + 16, 16)
        return {"sp_0": s // 4, "sp_1": lax.rem(s, 4)}

    used = [0]
    started = []

    def send(src, dst, device):
        i = used[0]
        used[0] += 1
        copy = pltpu.make_async_remote_copy(
            src_ref=src, dst_ref=dst, send_sem=send_sem.at[i], recv_sem=recv_sem.at[i],
            device_id=device, device_id_type=MESH,
        )
        copy.start()
        started.append(copy)
        return copy

    loads = [
        pltpu.make_async_copy(w_hbm, wbuf.at[0, cc], local_sem.at[0]),
        pltpu.make_async_copy(v_hbm.at[0], v_s, local_sem.at[1]),
        pltpu.make_async_copy(g_hbm.at[0], g_s, local_sem.at[2]),
        pltpu.make_async_copy(u_hbm.at[0], u_s, local_sem.at[3]),
    ]
    for load in loads:
        load.start()

    barrier = pltpu.get_barrier_semaphore()
    pl.semaphore_signal(barrier, inc=1, device_id=sibling, device_id_type=MESH)
    for d in range(1, NZ):
        pl.semaphore_signal(barrier, inc=1, device_id=zdev(d), device_id_type=MESH)
    for d in range(1, 16):
        pl.semaphore_signal(barrier, inc=1, device_id=spdev(d), device_id_type=MESH)

    tapsb[sp, :TAPS] = taps_ref[...]
    tapsb[sp, TAPS:] = jnp.zeros((1, 128), F32)
    loads[0].wait()
    pl.semaphore_wait(barrier, 23)

    parity = lax.rem(cy + cx, 2)
    w_copies = {}
    w_quarters = {}
    w_pair = {}

    def w_send(step, sub):
        rows = pl.ds(pl.multiple_of(64 * parity + 32 * sub, 32), 32)
        lanes = (slice(0, 1024), slice(1024, 2048)) if step == 4 else (slice(None), slice(None))
        for way, sign in ((0, 1), (1, -1)):
            src = (-sign * (step - 1)) % NZ
            dst = (-sign * step) % NZ
            w_copies[step, sub, way] = send(
                wbuf.at[src, cc, rows, lanes[way]], wbuf.at[dst, cc, rows, lanes[way]], zdev(sign)
            )

    def w_share(rel):
        if rel:
            for turn in range(4):
                w_quarters[rel, turn].wait_recv()
        w_pair[rel] = send(wbuf.at[rel, cc], wbuf.at[rel, cc], sibling)

    def w_event(step, sub):
        for way in (0, 1):
            w_copies[step, sub, way].wait_recv()
        if step < 4:
            w_send(step + 1, sub)
        name, at = (("sp_1", cx), ("sp_0", cy))[sub]
        for rel in sorted({step, (-step) % NZ}):
            for turn, sign in ((2 * sub, 1), (2 * sub + 1, -1)):
                rows = pl.ds(pl.multiple_of(64 * parity + 16 * turn, 16), 16)
                w_quarters[rel, turn] = send(
                    wbuf.at[rel, cc, rows], wbuf.at[rel, cc, rows], {name: lax.rem(at + sign + 4, 4)}
                )

    taps_copies = [send(tapsb.at[sp], tapsb.at[sp], spdev(d)) for d in range(1, 16)]
    w_send(1, 0)
    w_send(1, 1)
    for load in loads[1:]:
        load.wait()
    u_copy = send(u_s, usib, sibling)
    w_share(0)

    def glu_rows(r):
        rows = pl.ds(r, 32)
        for c in range(NC):
            lanes = slice(128 * c, 128 * c + 128)
            value = v_s[rows, lanes].astype(F32)
            sig = jax.nn.sigmoid(g_s[rows, lanes].astype(F32))
            wide = value * sig
            gate_a[c, rows, :] = sig
            gate_b[c, rows, :] = wide * (1.0 - sig)
            narrow = wide.astype(BF16)
            glu[c, pl.ds(r + 32, 32), :] = narrow.astype(F32)
            yield lanes, narrow

    for lanes, narrow in glu_rows(TOK - 32):
        halo_out[:, lanes] = narrow
    halo_copy = send(halo_out, halo_in, spdev(1))

    def glu_step(i, carry):
        for _ in glu_rows(pl.multiple_of(i * 32, 32)):
            pass
        return carry

    lax.fori_loop(0, TOK // 32 - 1, glu_step, 0)

    for copy in taps_copies:
        copy.wait_recv()

    mean_s[...] = jnp.zeros_like(mean_s)

    def conv_chunk(first, last, c, carry):
        taps = [jnp.broadcast_to(tapsb[c, j : j + 1, :], (8, 128)) for j in range(TAPS)]

        def rows_step(i, carry):
            for k in range(8):
                r = pl.multiple_of(i * 64, 64) + 8 * k
                parts = [None] * 2
                for j in range(TAPS):
                    term = taps[j] * glu[c, pl.ds(r + 2 + j, 8), :]
                    parts[j % 2] = term if parts[j % 2] is None else parts[j % 2] + term
                total = (parts[0] + parts[1]).astype(BF16).astype(F32)
                conv[c, pl.ds(r, 8), :] = total
                mean_s[pl.ds(r, 8), :] += total
            return carry

        return lax.fori_loop(first, last, rows_step, carry)

    body_rows = functools.partial(conv_chunk, 1, TOK // 64)
    w_event(1, 0)
    lax.fori_loop(0, 8, body_rows, 0)
    w_event(1, 1)
    lax.fori_loop(8, NC, body_rows, 0)
    w_event(2, 0)
    halo_copy.wait_recv()
    keep = (sp > 0).astype(F32)
    for c in range(NC):
        glu[c, 0:32, :] = halo_in[:, 128 * c : 128 * c + 128].astype(F32) * keep
    lax.fori_loop(0, NC, functools.partial(conv_chunk, 0, 1), 0)

    def norm_step(i, carry):
        rows = pl.ds(pl.multiple_of(i * 32, 32), 32)
        mu = jnp.broadcast_to(jnp.sum(mean_s[rows, :], axis=1, keepdims=True) * (1.0 / CH), (32, 128))
        squares = jnp.zeros((32, 128), F32)
        for c in range(NC):
            centered = conv[c, rows, :] - mu
            squares = squares + centered * centered
        inv = lax.rsqrt(jnp.sum(squares, axis=1, keepdims=True) * (1.0 / CH) + NORM_EPS)
        inv = jnp.broadcast_to(inv, (32, 128))
        mean_s[rows, :] = mu
        inv_s[rows, :] = inv
        for c in range(NC):
            lanes = slice(128 * c, 128 * c + 128)
            scaled = (conv[c, rows, :] - mu) * inv * gain_ref[:, lanes]
            act[rows, lanes] = (scaled * jax.nn.sigmoid(scaled)).astype(BF16)
        return carry

    act_copies = []
    for part_at in range(4):
        lax.fori_loop(2 * part_at, 2 * part_at + 2, norm_step, 0)
        rows = pl.ds(64 * part_at, 64)
        act_copies.append(send(act.at[rows], actsib.at[rows], sibling))
    w_event(2, 1)
    u_copy.wait_recv()

    def transpose_step(k, carry):
        zb = lax.rem(cz + k, NZ)
        cols = pl.ds(pl.multiple_of(zb * 256 + cc * 128, 128), 128)
        ut[k, :, 0:256] = u_s[:, cols].T
        ut[k, :, 256:512] = usib[:, cols].T
        return carry

    lax.fori_loop(0, NZ, transpose_step, 0)

    w_share(1)
    w_share(7)
    for copy in act_copies:
        copy.wait_recv()

    axes = ((("sp_1", cx), ("sp_0", cy)), (("sp_0", cy), ("sp_1", cx)))

    def near(axis, d):
        name, at = axis
        return {name: lax.rem(at + d + 4, 4)}

    def part(axis, d):
        return lax.rem(axis[1] + d + 4, 4)

    def partial_sums(stage):
        for k in range(NZ):
            lhs = ut[k]
            for n in range(2):
                lanes = slice(1024 * stage + 512 * n, 1024 * stage + 512 * n + 512)
                total = jnp.dot(lhs[:, 0:256], act[:, lanes], preferred_element_type=F32)
                total = total + jnp.dot(lhs[:, 256:512], actsib[:, lanes], preferred_element_type=F32)
                narrow = total.astype(BF16)
                for h in range(2):
                    for p in range(4):
                        first = 64 * h + 16 * p
                        pbuf[stage, h, p, k, :, 512 * n : 512 * n + 512] = narrow[first : first + 16, :]

    rs_copies = {}

    def rs1_send(stage):
        for h in range(2):
            axis = axes[h][0]
            far = part(axis, 2)
            for way, sign, lanes in ((0, 1, slice(0, 512)), (1, -1, slice(512, 1024))):
                rs_copies[1, stage, h, way] = send(
                    pbuf.at[stage, h, far, :, :, lanes], r1.at[stage, h, way], near(axis, sign)
                )

    def rs1_mid(stage):
        for h in range(2):
            axis = axes[h][0]
            for way, sign, lanes in ((0, 1, slice(0, 512)), (1, -1, slice(512, 1024))):
                rs_copies[1, stage, h, way].wait_recv()
                to = part(axis, sign)

                def add(k, carry, h=h, to=to, way=way, lanes=lanes):
                    pbuf[stage, h, to, k, :, lanes] = (
                        pbuf[stage, h, to, k, :, lanes].astype(F32) + r1[stage, h, way, k].astype(F32)
                    ).astype(BF16)
                    return carry

                lax.fori_loop(0, NZ, add, 0)
                rs_copies[2, stage, h, way] = send(
                    pbuf.at[stage, h, to], r2.at[stage, h, way], near(axis, sign)
                )

    def rs1_fin(stage):
        for h in range(2):
            mine = part(axes[h][0], 0)
            axis = axes[h][1]
            for way in (0, 1):
                rs_copies[2, stage, h, way].wait_recv()

            def add(k, carry, h=h, mine=mine):
                for p in range(4):
                    lanes = slice(256 * p, 256 * p + 256)
                    q[stage, h, p, k] = (
                        pbuf[stage, h, mine, k, :, lanes].astype(F32)
                        + r2[stage, h, 0, k, :, lanes].astype(F32)
                        + r2[stage, h, 1, k, :, lanes].astype(F32)
                    ).astype(BF16)
                return carry

            lax.fori_loop(0, NZ, add, 0)
            far = part(axis, 2)
            for way, sign, lanes in ((0, 1, slice(0, 128)), (1, -1, slice(128, 256))):
                rs_copies[3, stage, h, way] = send(
                    q.at[stage, h, far, :, :, lanes], s1.at[stage, h, way], near(axis, sign)
                )

    def rs2_mid(stage):
        for h in range(2):
            axis = axes[h][1]
            for way, sign, lanes in ((0, 1, slice(0, 128)), (1, -1, slice(128, 256))):
                rs_copies[3, stage, h, way].wait_recv()
                to = part(axis, sign)
                for k in range(NZ):
                    q[stage, h, to, k, :, lanes] = (
                        q[stage, h, to, k, :, lanes].astype(F32) + s1[stage, h, way, k].astype(F32)
                    ).astype(BF16)
                rs_copies[4, stage, h, way] = send(
                    q.at[stage, h, to], s2.at[stage, h, way], near(axis, sign)
                )

    z_copies = {}

    def rs2_fin(stage):
        for h in range(2):
            mine = part(axes[h][1], 0)
            for way in (0, 1):
                rs_copies[4, stage, h, way].wait_recv()
            for k in range(NZ):
                vz[stage, k, h] = (
                    q[stage, h, mine, k].astype(F32)
                    + s2[stage, h, 0, k].astype(F32)
                    + s2[stage, h, 1, k].astype(F32)
                ).astype(BF16)
        for k in (4, 3, 5, 2, 6, 1, 7):
            z_copies[stage, k] = send(vz.at[stage, k], rz.at[stage, k], zdev(k))

    gather_copies = []

    def rs3(stage):
        total = vz[stage, 0].astype(F32)
        for k in range(1, NZ):
            z_copies[stage, k].wait_recv()
            total = total + rz[stage, k].astype(F32)
        fg[stage, sp] = total.astype(BF16)
        for d in range(1, 16):
            gather_copies.append(send(fg.at[stage, sp], fg.at[stage, sp], spdev(d)))

    def grad_block(rels, first=False):
        for rel in rels:
            w_pair[rel].wait_recv()
        lhs = []
        for rel in rels:
            zb = lax.rem(cz + rel, NZ)
            lhs.append(u_s[:, pl.ds(pl.multiple_of(zb * 256, 256), 256)])

        def step(n, carry):
            lanes = pl.ds(pl.multiple_of(n * 512, 512), 512)
            total = None
            for left, rel in zip(lhs, rels):
                right = wbuf[rel, :, :, lanes].reshape(256, 512)
                term = jnp.dot(left, right, preferred_element_type=F32)
                total = term if total is None else total + term
            if first:
                gacc[:, lanes] = total
            else:
                gacc[:, lanes] += total
            return carry

        lax.fori_loop(0, 4, step, 0)

    partial_sums(0)
    rs1_send(0)
    w_event(3, 0)
    partial_sums(1)
    rs1_send(1)
    w_event(3, 1)
    w_event(4, 0)
    grad_block((0, 1, 7), first=True)
    w_event(4, 1)
    rs1_mid(0)
    w_share(2)
    w_share(6)
    rs1_mid(1)
    w_share(3)
    w_share(5)
    grad_block((2, 6))
    w_share(4)
    grad_block((3, 5))
    rs1_fin(0)
    grad_block((4,))

    dn[...] = jnp.zeros_like(dn)

    def back_rows(r):
        rows = pl.ds(r, 32)
        mu = mean_s[rows, :]
        inv = inv_s[rows, :]
        sum1 = jnp.zeros((32, 128), F32)
        sum2 = jnp.zeros((32, 128), F32)
        for c in range(NC):
            lanes = slice(128 * c, 128 * c + 128)
            gain = gain_ref[:, lanes]
            normed = (conv[c, rows, :] - mu) * inv
            scaled = normed * gain
            sig = jax.nn.sigmoid(scaled)
            grad_scaled = gacc[rows, lanes] * sig * (1.0 + scaled * (1.0 - sig))
            gain_term = grad_scaled * normed
            dn[c] += (gain_term[0:8] + gain_term[8:16]) + (gain_term[16:24] + gain_term[24:32])
            grad_normed = grad_scaled * gain
            gacc[rows, lanes] = grad_normed
            sum1 = sum1 + grad_normed
            sum2 = sum2 + grad_normed * normed
        m1 = jnp.broadcast_to(jnp.sum(sum1, axis=1, keepdims=True) * (1.0 / CH), (32, 128))
        m2 = jnp.broadcast_to(jnp.sum(sum2, axis=1, keepdims=True) * (1.0 / CH), (32, 128))
        for c in range(NC):
            lanes = slice(128 * c, 128 * c + 128)
            normed = (conv[c, rows, :] - mu) * inv
            narrow = (inv * (gacc[rows, lanes] - m1 - normed * m2)).astype(BF16)
            gpad[c, rows, :] = narrow.astype(F32)
            yield lanes, narrow

    for lanes, narrow in back_rows(0):
        ghalo_out[:, lanes] = narrow
    ghalo_copy = send(ghalo_out, ghalo_in, spdev(-1))

    def back_step(i, carry):
        for _ in back_rows(pl.multiple_of(i * 32, 32)):
            pass
        return carry

    lax.fori_loop(1, TOK // 32, back_step, 0)

    def taps_chunk(c, carry):
        def rows_step(i, sums):
            sums = list(sums)
            for k in range(4):
                r = pl.multiple_of(i * 32, 32) + 8 * k
                g = gpad[c, pl.ds(r, 8), :]
                for j in range(TAPS):
                    sums[j] = sums[j] + g * glu[c, pl.ds(r + 2 + j, 8), :]
            return tuple(sums)

        sums = lax.fori_loop(0, TOK // 32, rows_step, tuple(jnp.zeros((8, 128), F32) for _ in range(TAPS)))
        for j in range(TAPS):
            tg[c, j : j + 1, :] = jnp.sum(sums[j], axis=0, keepdims=True)
        tg[c, TAPS:, :] = jnp.sum(dn[c], axis=0, keepdims=True)
        return carry

    rs1_fin(1)
    lax.fori_loop(0, 4, taps_chunk, 0)
    rs2_mid(0)
    lax.fori_loop(4, 8, taps_chunk, 0)
    rs2_mid(1)
    lax.fori_loop(8, 12, taps_chunk, 0)
    rs2_fin(0)
    lax.fori_loop(12, NC, taps_chunk, 0)
    part_copies = [send(tg.at[lax.rem(sp + d, 16)], tr.at[d], spdev(d)) for d in range(1, 16)]
    rs2_fin(1)

    ghalo_copy.wait_recv()
    keep_g = (sp < 15).astype(F32)
    for c in range(NC):
        gpad[c, TOK:, :] = ghalo_in[:, 128 * c : 128 * c + 128].astype(F32) * keep_g

    def grad_chunk(c, carry):
        taps = [jnp.broadcast_to(tapsb[c, j : j + 1, :], (8, 128)) for j in range(TAPS)]
        lanes = pl.ds(pl.multiple_of(c * 128, 128), 128)

        def rows_step(i, carry):
            base = pl.multiple_of(i * 64, 64)
            for pair in range(4):
                values, gates = [], []
                for k in (2 * pair, 2 * pair + 1):
                    r = base + 8 * k
                    parts = [None] * 2
                    for j in range(TAPS):
                        term = taps[j] * gpad[c, pl.ds(r + 30 - j, 8), :]
                        parts[j % 2] = term if parts[j % 2] is None else parts[j % 2] + term
                    total = (parts[0] + parts[1]).astype(BF16).astype(F32)
                    values.append(total * gate_a[c, pl.ds(r, 8), :])
                    gates.append(total * gate_b[c, pl.ds(r, 8), :])
                rows = pl.ds(base + 16 * pair, 16)
                gv_s[rows, lanes] = jnp.concatenate(values, axis=0).astype(BF16)
                gt_s[rows, lanes] = jnp.concatenate(gates, axis=0).astype(BF16)
            return carry

        return lax.fori_loop(0, TOK // 64, rows_step, carry)

    stores = []

    def grad_group(at):
        lax.fori_loop(4 * at, 4 * at + 4, grad_chunk, 0)
        lanes = pl.ds(512 * at, 512)
        for narrow, wide in ((gv_s, gv_hbm), (gt_s, gt_hbm)):
            copy = pltpu.make_async_copy(
                narrow.at[:, lanes], wide.at[0, :, lanes], local_sem.at[4 + len(stores)]
            )
            copy.start()
            stores.append(copy)

    grad_group(0)
    total = tg[sp]
    for d in range(1, 16):
        part_copies[d - 1].wait_recv()
        total = total + tr[d]
    tz[cz] = total
    tz_copies = [send(tz.at[cz], tz.at[cz], zdev(d)) for d in range(1, NZ)]
    grad_group(1)
    rs3(0)
    grad_group(2)
    rs3(1)
    grad_group(3)

    for copy in tz_copies:
        copy.wait_recv()
    total = tz[0]
    for k in range(1, NZ):
        total = total + tz[k]
    tfin[...] = total
    pair_copy = send(tfin, tsib, sibling)
    pair_copy.wait_recv()
    total = tfin[...] + tsib[...]
    dt_ref[...] = total[:TAPS]
    gfull[sp] = jnp.broadcast_to(total[TAPS:, :], (8, 128))
    gain_copies = [send(gfull.at[sp], gfull.at[sp], spdev(d)) for d in range(1, 16)]

    for copy in gather_copies:
        copy.wait_recv()
    for s in range(16):
        y, x = divmod(s, 4)
        for t in range(2):
            lane = 1024 * t + 256 * y
            gw_ref[16 * x : 16 * x + 16, lane : lane + 256] = fg[t, s, 0]
            lane = 1024 * t + 256 * x
            gw_ref[64 + 16 * y : 80 + 16 * y, lane : lane + 256] = fg[t, s, 1]
    for copy in gain_copies:
        copy.wait_recv()
    for c in range(NC):
        dn_ref[:, 128 * c : 128 * c + 128] = gfull[c, 0:1, :]
    for copy in stores:
        copy.wait()
    for copy in started:
        copy.wait_send()


def body(value_half, gate_half, upstream, conv_taps, norm_gain, out_weight):
    vmem = pl.BlockSpec(memory_space=pltpu.VMEM)
    hbm = pl.BlockSpec(memory_space=pl.ANY)
    grad_value, grad_gate, grad_rows, taps, gain = pl.pallas_call(
        kernel,
        out_shape=(
            jax.ShapeDtypeStruct((1, TOK, CH), BF16),
            jax.ShapeDtypeStruct((1, TOK, CH), BF16),
            jax.ShapeDtypeStruct((128, CH), BF16),
            jax.ShapeDtypeStruct((TAPS, 128), F32),
            jax.ShapeDtypeStruct((1, CH), F32),
        ),
        in_specs=[hbm] * 4 + [vmem] * 2,
        out_specs=[hbm] * 2 + [vmem] * 3,
        scratch_shapes=[
            pltpu.VMEM((TOK, CH), BF16),
            pltpu.VMEM((TOK, CH), BF16),
            pltpu.VMEM((TOK, CH), BF16),
            pltpu.VMEM((TOK, CH), BF16),
            pltpu.VMEM((NZ, 2, 128, CH), BF16),
            pltpu.VMEM((NC, 32, 128), F32),
            pltpu.VMEM((NC, TOK + 32, 128), F32),
            pltpu.VMEM((NC, TOK, 128), F32),
            pltpu.VMEM((TOK, CH), BF16),
            pltpu.VMEM((TOK, CH), BF16),
            pltpu.VMEM((NZ, 128, 512), BF16),
            pltpu.VMEM((2, 2, 4, NZ, 16, 1024), BF16),
            pltpu.VMEM((2, 2, 2, NZ, 16, 512), BF16),
            pltpu.VMEM((2, 2, 2, NZ, 16, 1024), BF16),
            pltpu.VMEM((2, 2, 4, NZ, 16, 256), BF16),
            pltpu.VMEM((2, 2, 2, NZ, 16, 128), BF16),
            pltpu.VMEM((2, 2, 2, NZ, 16, 256), BF16),
            pltpu.VMEM((2, NZ, 2, 16, 256), BF16),
            pltpu.VMEM((2, NZ, 2, 16, 256), BF16),
            pltpu.VMEM((2, 16, 2, 16, 256), BF16),
            pltpu.VMEM((TOK, CH), F32),
            pltpu.VMEM((NC, TOK + 32, 128), F32),
            pltpu.VMEM((TOK, 128), F32),
            pltpu.VMEM((TOK, 128), F32),
            pltpu.VMEM((NC, TOK, 128), F32),
            pltpu.VMEM((NC, TOK, 128), F32),
            pltpu.VMEM((TOK, CH), BF16),
            pltpu.VMEM((TOK, CH), BF16),
            pltpu.VMEM((32, CH), BF16),
            pltpu.VMEM((32, CH), BF16),
            pltpu.VMEM((32, CH), BF16),
            pltpu.VMEM((32, CH), BF16),
            pltpu.VMEM((NC, 8, 128), F32),
            pltpu.VMEM((NC, 32, 128), F32),
            pltpu.VMEM((16, 32, 128), F32),
            pltpu.VMEM((NZ, 32, 128), F32),
            pltpu.VMEM((32, 128), F32),
            pltpu.VMEM((32, 128), F32),
            pltpu.VMEM((16, 8, 128), F32),
            pltpu.SemaphoreType.DMA((12,)),
            pltpu.SemaphoreType.DMA((N_SEND,)),
            pltpu.SemaphoreType.DMA((N_SEND,)),
        ],
        compiler_params=pltpu.CompilerParams(
            collective_id=0, has_side_effects=True, vmem_limit_bytes=66_000_000
        ),
    )(value_half, gate_half, upstream, out_weight, conv_taps, norm_gain[None])
    return grad_value, grad_gate, taps, gain.reshape(CH), grad_rows.astype(F32)


def solution(mesh):
    torus = Mesh(mesh.devices.reshape(4, 4, 8, 2), ("sp_0", "sp_1", "dp_0", "dp_1"))
    placed = (P(DP, SP, None), P(DP, SP, None), P(DP, SP, None), P(None, SP), P(), P(DP, None))
    return jax.shard_map(
        body,
        mesh=torus,
        in_specs=placed,
        out_specs=(P(DP, SP, None), P(DP, SP, None), P(None, SP), P(), P(DP, None)),
        check_vma=False,
    )
```

time: 111 us -> 90 us (0.81)
  Pallas kernels: 103 us -> 83 us
  other arithmetic: 5.36 us -> 2.21 us
  local copies, waits for them, and re-layouts: 2.05 us -> 3.88 us
    pallas_call x1, Pallas kernels: 103 us -> 83 us  [body(): pl.pallas_call(kernel, out_shape=(jax.ShapeDtypeStruct((1, TOK, CH), BF16...]
    convert_element_type x1 -> x0, other arithmetic: 4.29 us -> none  [body(): (wide * value_half.astype(F32) * sig_gate * (1.0 - sig_gate)).astype(BF16)]
    unnamed x5 -> x12, local copies, waits for them, and re-layouts: 0.61 us -> 3.88 us
    slice x1 -> x0, local copies, waits for them, and re-layouts: 1.44 us -> none  [body(): gain[:, 0, :].reshape(CH)]
    convert_element_type x1, other arithmetic: 1.07 us -> 2.21 us  [body(): grad_rows.astype(F32)]
where the time goes in v2:
time: 90 us; the launch traced here: 89.7 us
  Pallas kernels  83 us (92%)
  local copies, waits for them, and re-layouts  3.88 us (4%)
  other arithmetic  2.21 us (2%)
    pallas_call x1, Pallas kernels, body(): pl.pallas_call(kernel, out_shape=(jax.ShapeDtypeStruct((1, TOK, CH), BF16...  83 us
    unnamed x12, local copies, waits for them, and re-layouts  3.88 us
    convert_element_type x1, other arithmetic, body(): grad_rows.astype(F32)  2.21 us

profile of v2, /device:TPU:1, one launch (start us, length us, event | category | flops | bytes accessed | tf_op | source)
XLA Modules:
  0.0 89.7 jit_solution(16292030920507335155)
XLA Ops:
  0.6 83.0 %shard_map.101 = (bf16[1,256,2048]{2,1,0:T(8,128)(2,1)}, bf16[1,256,2048]{2,1,0:T(8,128)(2,1)}, bf16[128,2048]{1,0:T(8,128)(2,1)}, f32[31,128]{1,0:T(8,128)}, f32[1,2048]{1,0:T(1,128)}) custom-call(bf16[1,256,2048]{2,1,0:T(8,128)(2,1)} %v_hbm.1, bf16[1,256,2048]{2,1,0:T(8,128)(2,1)} %g_hbm.1, bf16[1,256,2048]{2,1,0:T(8,128)(2,1)} %u_hbm.1, ...), custom_call_target="tpu_custom_call" | custom-call | tf_op jit(solution)/shard_map/pallas_call | solution.py:537
  83.6 0.0 copy-start.1
  83.7 2.2 %convert_element_type.3 = f32[128,2048]{1,0:T(8,128)} convert(bf16[128,2048]{1,0:T(8,128)(2,1)} %get-tuple-element.14) | non-fusion elementwise | flops 262144 | bytes 1572864 | tf_op jit(solution)/shard_map/convert_element_type | solution.py:596
  85.9 0.0 copy-done.1
  85.9 0.0 copy-start
  85.9 1.0 %copy.15 = bf16[1,256,2048]{2,1,0:T(8,128)(2,1)} copy(bf16[1,256,2048]{2,1,0:T(8,128)(2,1)S(1)} %copy-done.1) | data formatting | bytes 2097152
  86.8 0.6 copy-done
  87.5 0.0 copy-start.2
  87.5 1.0 %copy.16 = bf16[1,256,2048]{2,1,0:T(8,128)(2,1)} copy(bf16[1,256,2048]{2,1,0:T(8,128)(2,1)S(1)} %copy-done) | data formatting | bytes 2097152
  88.4 0.0 copy-done.2
  88.4 0.0 copy-start.3
  88.4 0.6 copy.17
  89.0 0.1 copy-done.3
  89.1 0.6 copy.18
Async XLA Ops:
  83.6 2.2 %copy-start.1 = (bf16[1,256,2048]{2,1,0:T(8,128)(2,1)S(1)}, bf16[1,256,2048]{2,1,0:T(8,128)(2,1)}, u32[]{:S(2)}) copy-start(bf16[1,256,2048]{2,1,0:T(8,128)(2,1)} %get-tuple-element.20) | copy-start | bytes 3145732
  85.9 1.6 %copy-start = (bf16[1,256,2048]{2,1,0:T(8,128)(2,1)S(1)}, bf16[1,256,2048]{2,1,0:T(8,128)(2,1)}, u32[]{:S(2)}) copy-start(bf16[1,256,2048]{2,1,0:T(8,128)(2,1)} %get-tuple-element.21) | copy-start | bytes 3145732
  87.5 1.0 %copy-start.2 = (f32[31,128]{1,0:T(8,128)S(1)}, f32[31,128]{1,0:T(8,128)}, u32[]{:S(2)}) copy-start(f32[31,128]{1,0:T(8,128)} %get-tuple-element.22) | copy-start | bytes 47620
  88.4 0.7 copy-start.3

commit v3 on v2

--- a/solution.py
+++ b/solution.py
@@ -19,8 +19,10 @@
 CH = 2048
 NC = CH // 128
 TAPS = 31
+ROW_ORDER = (0, 1, 3, 2)
 NZ = 8
-N_SEND = 220
+NS = 4
+N_SEND = 320
 
 
 def kernel(
@@ -28,7 +30,7 @@
     gv_hbm, gt_hbm, gw_ref, dt_ref, dn_ref,
     v_s, g_s, u_s, usib, wbuf, tapsb, glu, conv, act, actsib, ut,
     pbuf, r1, r2, q, s1, s2, vz, rz, fg, gacc, gpad, mean_s, inv_s, gate_a, gate_b, gv_s, gt_s,
-    halo_out, halo_in, ghalo_out, ghalo_in, dn, tg, tr, tz, tsib, tfin, gfull,
+    halo_out, halo_in, ghalo_out, ghalo_in, dn, tg, tr, tz, tsib, tfin, gfull, dr, dz, dfin, dsib,
     local_sem, send_sem, recv_sem,
 ):
     cy, cx, cz, cc = (lax.axis_index(a) for a in ("sp_0", "sp_1", "dp_0", "dp_1"))
@@ -83,38 +85,62 @@
     w_quarters = {}
     w_pair = {}
 
-    def w_send(step, sub):
-        rows = pl.ds(pl.multiple_of(64 * parity + 32 * sub, 32), 32)
+    def arrived(copies, key):
+        copy = copies.pop(key, None)
+        if copy is not None:
+            copy.wait_recv()
+
+    def w_send(half, step, sub):
+        at = parity if half == 0 else 1 - parity
+        rows = pl.ds(pl.multiple_of(64 * at + 32 * sub, 32), 32)
         lanes = (slice(0, 1024), slice(1024, 2048)) if step == 4 else (slice(None), slice(None))
         for way, sign in ((0, 1), (1, -1)):
             src = (-sign * (step - 1)) % NZ
             dst = (-sign * step) % NZ
-            w_copies[step, sub, way] = send(
+            w_copies[half, step, sub, way] = send(
                 wbuf.at[src, cc, rows, lanes[way]], wbuf.at[dst, cc, rows, lanes[way]], zdev(sign)
             )
 
     def w_share(rel):
-        if rel:
-            for turn in range(4):
-                w_quarters[rel, turn].wait_recv()
+        for turn in range(4):
+            arrived(w_quarters, (rel, turn))
         w_pair[rel] = send(wbuf.at[rel, cc], wbuf.at[rel, cc], sibling)
 
     def w_event(step, sub):
         for way in (0, 1):
-            w_copies[step, sub, way].wait_recv()
+            arrived(w_copies, (0, step, sub, way))
         if step < 4:
-            w_send(step + 1, sub)
+            w_send(0, step + 1, sub)
         name, at = (("sp_1", cx), ("sp_0", cy))[sub]
-        for rel in sorted({step, (-step) % NZ}):
-            for turn, sign in ((2 * sub, 1), (2 * sub + 1, -1)):
-                rows = pl.ds(pl.multiple_of(64 * parity + 16 * turn, 16), 16)
-                w_quarters[rel, turn] = send(
-                    wbuf.at[rel, cc, rows], wbuf.at[rel, cc, rows], {name: lax.rem(at + sign + 4, 4)}
-                )
-
-    taps_copies = [send(tapsb.at[sp], tapsb.at[sp], spdev(d)) for d in range(1, 16)]
-    w_send(1, 0)
-    w_send(1, 1)
+        if step < 3:
+            for rel in (step, NZ - step):
+                for turn, sign in ((2 * sub, 1), (2 * sub + 1, -1)):
+                    rows = pl.ds(pl.multiple_of(64 * parity + 16 * turn, 16), 16)
+                    w_quarters[rel, turn] = send(
+                        wbuf.at[rel, cc, rows], wbuf.at[rel, cc, rows], {name: lax.rem(at + sign + 4, 4)}
+                    )
+
+    def w_rest(step, sub):
+        if step == 2:
+            for rel in (2, 6):
+                for turn in (2 * sub, 2 * sub + 1):
+                    arrived(w_quarters, (rel, turn))
+        else:
+            for way in (0, 1):
+                arrived(w_copies, (1, step, sub, way))
+        if step < 4:
+            w_send(1, step + 1, sub)
+
+    taps_copies = {
+        dy: [
+            send(tapsb.at[sp], tapsb.at[sp], {"sp_0": lax.rem(cy + dy, 4), "sp_1": lax.rem(cx + dx, 4)})
+            for dx in range(4)
+            if dx or dy
+        ]
+        for dy in ROW_ORDER
+    }
+    w_send(0, 1, 0)
+    w_send(0, 1, 1)
     for load in loads[1:]:
         load.wait()
     u_copy = send(u_s, usib, sibling)
@@ -144,8 +170,16 @@
 
     lax.fori_loop(0, TOK // 32 - 1, glu_step, 0)
 
-    for copy in taps_copies:
-        copy.wait_recv()
+    u_copy.wait_recv()
+
+    def transpose_step(k, carry):
+        zb = lax.rem(cz + k, NZ)
+        cols = pl.ds(pl.multiple_of(zb * 256 + cc * 128, 128), 128)
+        ut[k, :, 0:256] = u_s[:, cols].T
+        ut[k, :, 256:512] = usib[:, cols].T
+        return carry
+
+    lax.fori_loop(0, NZ, transpose_step, 0)
 
     mean_s[...] = jnp.zeros_like(mean_s)
 
@@ -167,11 +201,19 @@
         return lax.fori_loop(first, last, rows_step, carry)
 
     body_rows = functools.partial(conv_chunk, 1, TOK // 64)
+
+    def conv_group(dy):
+        for copy in taps_copies[dy]:
+            copy.wait_recv()
+        row = lax.rem(cy - dy + 4, 4)
+        lax.fori_loop(4 * row, 4 * row + 4, body_rows, 0)
+
+    conv_group(ROW_ORDER[0])
     w_event(1, 0)
-    lax.fori_loop(0, 8, body_rows, 0)
+    conv_group(ROW_ORDER[1])
+    conv_group(ROW_ORDER[2])
     w_event(1, 1)
-    lax.fori_loop(8, NC, body_rows, 0)
-    w_event(2, 0)
+    conv_group(ROW_ORDER[3])
     halo_copy.wait_recv()
     keep = (sp > 0).astype(F32)
     for c in range(NC):
@@ -196,22 +238,17 @@
         return carry
 
     act_copies = []
-    for part_at in range(4):
-        lax.fori_loop(2 * part_at, 2 * part_at + 2, norm_step, 0)
-        rows = pl.ds(64 * part_at, 64)
+
+    def norm_part(at):
+        lax.fori_loop(2 * at, 2 * at + 2, norm_step, 0)
+        rows = pl.ds(64 * at, 64)
         act_copies.append(send(act.at[rows], actsib.at[rows], sibling))
-    w_event(2, 1)
-    u_copy.wait_recv()
-
-    def transpose_step(k, carry):
-        zb = lax.rem(cz + k, NZ)
-        cols = pl.ds(pl.multiple_of(zb * 256 + cc * 128, 128), 128)
-        ut[k, :, 0:256] = u_s[:, cols].T
-        ut[k, :, 256:512] = usib[:, cols].T
-        return carry
-
-    lax.fori_loop(0, NZ, transpose_step, 0)
-
+
+    norm_part(0)
+    norm_part(1)
+    w_event(2, 0)
+    norm_part(2)
+    norm_part(3)
     w_share(1)
     w_share(7)
     for copy in act_copies:
@@ -227,17 +264,16 @@
         return lax.rem(axis[1] + d + 4, 4)
 
     def partial_sums(stage):
+        lanes = slice(512 * stage, 512 * stage + 512)
         for k in range(NZ):
             lhs = ut[k]
-            for n in range(2):
-                lanes = slice(1024 * stage + 512 * n, 1024 * stage + 512 * n + 512)
-                total = jnp.dot(lhs[:, 0:256], act[:, lanes], preferred_element_type=F32)
-                total = total + jnp.dot(lhs[:, 256:512], actsib[:, lanes], preferred_element_type=F32)
-                narrow = total.astype(BF16)
-                for h in range(2):
-                    for p in range(4):
-                        first = 64 * h + 16 * p
-                        pbuf[stage, h, p, k, :, 512 * n : 512 * n + 512] = narrow[first : first + 16, :]
+            total = jnp.dot(lhs[:, 0:256], act[:, lanes], preferred_element_type=F32)
+            total = total + jnp.dot(lhs[:, 256:512], actsib[:, lanes], preferred_element_type=F32)
+            narrow = total.astype(BF16)
+            for h in range(2):
+                for p in range(4):
+                    first = 64 * h + 16 * p
+                    pbuf[stage, h, p, k] = narrow[first : first + 16, :]
 
     rs_copies = {}
 
@@ -245,7 +281,7 @@
         for h in range(2):
             axis = axes[h][0]
             far = part(axis, 2)
-            for way, sign, lanes in ((0, 1, slice(0, 512)), (1, -1, slice(512, 1024))):
+            for way, sign, lanes in ((0, 1, slice(0, 256)), (1, -1, slice(256, 512))):
                 rs_copies[1, stage, h, way] = send(
                     pbuf.at[stage, h, far, :, :, lanes], r1.at[stage, h, way], near(axis, sign)
                 )
@@ -253,7 +289,7 @@
     def rs1_mid(stage):
         for h in range(2):
             axis = axes[h][0]
-            for way, sign, lanes in ((0, 1, slice(0, 512)), (1, -1, slice(512, 1024))):
+            for way, sign, lanes in ((0, 1, slice(0, 256)), (1, -1, slice(256, 512))):
                 rs_copies[1, stage, h, way].wait_recv()
                 to = part(axis, sign)
 
@@ -277,7 +313,7 @@
 
             def add(k, carry, h=h, mine=mine):
                 for p in range(4):
-                    lanes = slice(256 * p, 256 * p + 256)
+                    lanes = slice(128 * p, 128 * p + 128)
                     q[stage, h, p, k] = (
                         pbuf[stage, h, mine, k, :, lanes].astype(F32)
                         + r2[stage, h, 0, k, :, lanes].astype(F32)
@@ -287,20 +323,20 @@
 
             lax.fori_loop(0, NZ, add, 0)
             far = part(axis, 2)
-            for way, sign, lanes in ((0, 1, slice(0, 128)), (1, -1, slice(128, 256))):
+            for way, sign in ((0, 1), (1, -1)):
                 rs_copies[3, stage, h, way] = send(
-                    q.at[stage, h, far, :, :, lanes], s1.at[stage, h, way], near(axis, sign)
+                    q.at[stage, h, far, pl.ds(4 * way, 4)], s1.at[stage, h, way], near(axis, sign)
                 )
 
     def rs2_mid(stage):
         for h in range(2):
             axis = axes[h][1]
-            for way, sign, lanes in ((0, 1, slice(0, 128)), (1, -1, slice(128, 256))):
+            for way, sign in ((0, 1), (1, -1)):
                 rs_copies[3, stage, h, way].wait_recv()
                 to = part(axis, sign)
-                for k in range(NZ):
-                    q[stage, h, to, k, :, lanes] = (
-                        q[stage, h, to, k, :, lanes].astype(F32) + s1[stage, h, way, k].astype(F32)
+                for k in range(4):
+                    q[stage, h, to, 4 * way + k] = (
+                        q[stage, h, to, 4 * way + k].astype(F32) + s1[stage, h, way, k].astype(F32)
                     ).astype(BF16)
                 rs_copies[4, stage, h, way] = send(
                     q.at[stage, h, to], s2.at[stage, h, way], near(axis, sign)
@@ -358,23 +394,40 @@
 
     partial_sums(0)
     rs1_send(0)
-    w_event(3, 0)
+    w_event(2, 1)
     partial_sums(1)
     rs1_send(1)
+    w_rest(2, 0)
+    partial_sums(2)
+    rs1_send(2)
+    w_event(3, 0)
+    partial_sums(3)
+    rs1_send(3)
+    grad_block((0, 1, 7), first=True)
+    rs1_mid(0)
+    w_rest(2, 1)
     w_event(3, 1)
-    w_event(4, 0)
-    grad_block((0, 1, 7), first=True)
-    w_event(4, 1)
-    rs1_mid(0)
+    rs1_mid(1)
     w_share(2)
     w_share(6)
-    rs1_mid(1)
+    grad_block((2, 6))
+    w_rest(3, 0)
+    w_event(4, 0)
+    w_event(4, 1)
+    w_rest(3, 1)
+    rs1_fin(0)
+    rs1_mid(2)
     w_share(3)
     w_share(5)
-    grad_block((2, 6))
+    rs1_fin(1)
+    rs1_mid(3)
+    rs2_mid(0)
+    grad_block((3, 5))
+    w_rest(4, 0)
+    w_rest(4, 1)
     w_share(4)
-    grad_block((3, 5))
-    rs1_fin(0)
+    rs2_mid(1)
+    rs1_fin(2)
     grad_block((4,))
 
     dn[...] = jnp.zeros_like(dn)
@@ -418,6 +471,33 @@
 
     lax.fori_loop(1, TOK // 32, back_step, 0)
 
+    def rest_of_plane(d):
+        return lax.rem(sp + d, 16)
+
+    gain_copies = [send(dn.at[rest_of_plane(d)], dr.at[d], spdev(d)) for d in range(1, 16)]
+
+    def gain_sum():
+        total = dn[sp]
+        for d in range(1, 16):
+            gain_copies[d - 1].wait_recv()
+            total = total + dr[d]
+        dz[cz] = total
+        return [send(dz.at[cz], dz.at[cz], zdev(d)) for d in range(1, NZ)]
+
+    def gain_pair(copies):
+        for copy in copies:
+            copy.wait_recv()
+        total = dz[0]
+        for k in range(1, NZ):
+            total = total + dz[k]
+        dfin[...] = total
+        return send(dfin, dsib, sibling)
+
+    def gain_out(copy):
+        copy.wait_recv()
+        gfull[sp] = dfin[...] + dsib[...]
+        return [send(gfull.at[sp], gfull.at[sp], spdev(d)) for d in range(1, 16)]
+
     def taps_chunk(c, carry):
         def rows_step(i, sums):
             sums = list(sums)
@@ -431,19 +511,36 @@
         sums = lax.fori_loop(0, TOK // 32, rows_step, tuple(jnp.zeros((8, 128), F32) for _ in range(TAPS)))
         for j in range(TAPS):
             tg[c, j : j + 1, :] = jnp.sum(sums[j], axis=0, keepdims=True)
-        tg[c, TAPS:, :] = jnp.sum(dn[c], axis=0, keepdims=True)
+        tg[c, TAPS:, :] = jnp.zeros((1, 128), F32)
         return carry
 
-    rs1_fin(1)
-    lax.fori_loop(0, 4, taps_chunk, 0)
-    rs2_mid(0)
-    lax.fori_loop(4, 8, taps_chunk, 0)
-    rs2_mid(1)
-    lax.fori_loop(8, 12, taps_chunk, 0)
+    part_copies = []
+
+    def taps_group(dy):
+        row = lax.rem(cy + dy, 4)
+        lax.fori_loop(4 * row, 4 * row + 4, taps_chunk, 0)
+        for dx in range(4):
+            if dx or dy:
+                x = lax.rem(cx + dx, 4)
+                part_copies.append(
+                    send(tg.at[4 * row + x], tr.at[4 * dy + dx], {"sp_0": row, "sp_1": x})
+                )
+
     rs2_fin(0)
-    lax.fori_loop(12, NC, taps_chunk, 0)
-    part_copies = [send(tg.at[lax.rem(sp + d, 16)], tr.at[d], spdev(d)) for d in range(1, 16)]
+    rs2_mid(2)
+    rs1_fin(3)
+    taps_group(2)
     rs2_fin(1)
+    taps_group(1)
+    gain_z = gain_sum()
+    rs2_mid(3)
+    rs2_fin(2)
+    taps_group(3)
+    rs2_fin(3)
+    rs3(0)
+    taps_group(0)
+    gain_last = gain_pair(gain_z)
+    rs3(1)
 
     ghalo_copy.wait_recv()
     keep_g = (sp < 15).astype(F32)
@@ -487,16 +584,18 @@
             stores.append(copy)
 
     grad_group(0)
+    gain_copies2 = gain_out(gain_last)
+    rs3(2)
+    grad_group(1)
     total = tg[sp]
+    for copy in part_copies:
+        copy.wait_recv()
     for d in range(1, 16):
-        part_copies[d - 1].wait_recv()
         total = total + tr[d]
     tz[cz] = total
     tz_copies = [send(tz.at[cz], tz.at[cz], zdev(d)) for d in range(1, NZ)]
-    grad_group(1)
-    rs3(0)
+    rs3(3)
     grad_group(2)
-    rs3(1)
     grad_group(3)
 
     for copy in tz_copies:
@@ -506,29 +605,47 @@
         total = total + tz[k]
     tfin[...] = total
     pair_copy = send(tfin, tsib, sibling)
-    pair_copy.wait_recv()
-    total = tfin[...] + tsib[...]
-    dt_ref[...] = total[:TAPS]
-    gfull[sp] = jnp.broadcast_to(total[TAPS:, :], (8, 128))
-    gain_copies = [send(gfull.at[sp], gfull.at[sp], spdev(d)) for d in range(1, 16)]
 
     for copy in gather_copies:
         copy.wait_recv()
     for s in range(16):
         y, x = divmod(s, 4)
-        for t in range(2):
-            lane = 1024 * t + 256 * y
-            gw_ref[16 * x : 16 * x + 16, lane : lane + 256] = fg[t, s, 0]
-            lane = 1024 * t + 256 * x
-            gw_ref[64 + 16 * y : 80 + 16 * y, lane : lane + 256] = fg[t, s, 1]
-    for copy in gain_copies:
+        for t in range(NS):
+            lane = 512 * t + 128 * y
+            gw_ref[16 * x : 16 * x + 16, lane : lane + 128] = fg[t, s, 0]
+            lane = 512 * t + 128 * x
+            gw_ref[64 + 16 * y : 80 + 16 * y, lane : lane + 128] = fg[t, s, 1]
+    for copy in gain_copies2:
         copy.wait_recv()
     for c in range(NC):
-        dn_ref[:, 128 * c : 128 * c + 128] = gfull[c, 0:1, :]
+        dn_ref[:, 128 * c : 128 * c + 128] = jnp.sum(gfull[c], axis=0, keepdims=True)
+    pair_copy.wait_recv()
+    dt_ref[...] = (tfin[...] + tsib[...])[:TAPS]
     for copy in stores:
         copy.wait()
     for copy in started:
         copy.wait_send()
+
+
+def write_out(gv, gt, gw, dt, dn, gv_out, gt_out, gw_out, dt_out, dn_out, gv_s, gt_s, gw_s, gw_wide, dt_s, dn_s, sem):
+    copies = []
+    for i, (source, held, target) in enumerate(
+        ((gw, gw_s, gw_out), (gv, gv_s, gv_out), (gt, gt_s, gt_out), (dt, dt_s, dt_out), (dn, dn_s, dn_out))
+    ):
+        copy = pltpu.make_async_copy(source, held, sem.at[0, i])
+        copy.start()
+        copies.append((copy, held, target))
+    outs = []
+    for i, (copy, held, target) in enumerate(copies):
+        copy.wait()
+        if i == 0:
+            gw_wide[...] = gw_s[...].astype(F32)
+            held = gw_wide
+        out = pltpu.make_async_copy(held, target, sem.at[1, i])
+        out.start()
+        outs.append(out)
+    for out in outs:
+        out.wait()
 
 
 def body(value_half, gate_half, upstream, conv_taps, norm_gain, out_weight):
@@ -557,15 +674,15 @@
             pltpu.VMEM((TOK, CH), BF16),
             pltpu.VMEM((TOK, CH), BF16),
             pltpu.VMEM((NZ, 128, 512), BF16),
-            pltpu.VMEM((2, 2, 4, NZ, 16, 1024), BF16),
-            pltpu.VMEM((2, 2, 2, NZ, 16, 512), BF16),
-            pltpu.VMEM((2, 2, 2, NZ, 16, 1024), BF16),
-            pltpu.VMEM((2, 2, 4, NZ, 16, 256), BF16),
-            pltpu.VMEM((2, 2, 2, NZ, 16, 128), BF16),
-            pltpu.VMEM((2, 2, 2, NZ, 16, 256), BF16),
-            pltpu.VMEM((2, NZ, 2, 16, 256), BF16),
-            pltpu.VMEM((2, NZ, 2, 16, 256), BF16),
-            pltpu.VMEM((2, 16, 2, 16, 256), BF16),
+            pltpu.VMEM((NS, 2, 4, NZ, 16, 512), BF16),
+            pltpu.VMEM((NS, 2, 2, NZ, 16, 256), BF16),
+            pltpu.VMEM((NS, 2, 2, NZ, 16, 512), BF16),
+            pltpu.VMEM((NS, 2, 4, NZ, 16, 128), BF16),
+            pltpu.VMEM((NS, 2, 2, 4, 16, 128), BF16),
+            pltpu.VMEM((NS, 2, 2, NZ, 16, 128), BF16),
+            pltpu.VMEM((NS, NZ, 2, 16, 128), BF16),
+            pltpu.VMEM((NS, NZ, 2, 16, 128), BF16),
+            pltpu.VMEM((NS, 16, 2, 16, 128), BF16),
             pltpu.VMEM((TOK, CH), F32),
             pltpu.VMEM((NC, TOK + 32, 128), F32),
             pltpu.VMEM((TOK, 128), F32),
@@ -585,6 +702,10 @@
             pltpu.VMEM((32, 128), F32),
             pltpu.VMEM((32, 128), F32),
             pltpu.VMEM((16, 8, 128), F32),
+            pltpu.VMEM((16, 8, 128), F32),
+            pltpu.VMEM((NZ, 8, 128), F32),
+            pltpu.VMEM((8, 128), F32),
+            pltpu.VMEM((8, 128), F32),
             pltpu.SemaphoreType.DMA((12,)),
             pltpu.SemaphoreType.DMA((N_SEND,)),
             pltpu.SemaphoreType.DMA((N_SEND,)),
@@ -593,7 +714,29 @@
             collective_id=0, has_side_effects=True, vmem_limit_bytes=66_000_000
         ),
     )(value_half, gate_half, upstream, out_weight, conv_taps, norm_gain[None])
-    return grad_value, grad_gate, taps, gain.reshape(CH), grad_rows.astype(F32)
+    grad_value, grad_gate, grad_rows, taps, gain = pl.pallas_call(
+        write_out,
+        out_shape=(
+            jax.ShapeDtypeStruct((1, TOK, CH), BF16),
+            jax.ShapeDtypeStruct((1, TOK, CH), BF16),
+            jax.ShapeDtypeStruct((128, CH), F32),
+            jax.ShapeDtypeStruct((TAPS, 128), F32),
+            jax.ShapeDtypeStruct((1, CH), F32),
+        ),
+        in_specs=[hbm] * 5,
+        out_specs=[hbm] * 5,
+        scratch_shapes=[
+            pltpu.VMEM((1, TOK, CH), BF16),
+            pltpu.VMEM((1, TOK, CH), BF16),
+            pltpu.VMEM((128, CH), BF16),
+            pltpu.VMEM((128, CH), F32),
+            pltpu.VMEM((TAPS, 128), F32),
+            pltpu.VMEM((1, CH), F32),
+            pltpu.SemaphoreType.DMA((2, 5)),
+        ],
+        compiler_params=pltpu.CompilerParams(vmem_limit_bytes=60_000_000),
+    )(grad_value, grad_gate, grad_rows, taps, gain)
+    return grad_value, grad_gate, taps, gain.reshape(CH), grad_rows
 
 
 def solution(mesh):

time: 90 us -> 83.9 us (0.932)
  local copies, waits for them, and re-layouts: 3.88 us -> 0 us
  other arithmetic: 2.21 us -> 0 us
    unnamed x12 -> x0, local copies, waits for them, and re-layouts: 3.88 us -> none
    pallas_call x0 -> x1, Pallas kernels: none -> 2.86 us  [body(): pl.pallas_call(write_out, out_shape=(jax.ShapeDtypeStruct((1, TOK, CH), B...]
    pallas_call x1, Pallas kernels: 83 us -> 80.2 us  [body(): pl.pallas_call(kernel, out_shape=(jax.ShapeDtypeStruct((1, TOK, CH), BF16...]
    convert_element_type x1 -> x0, other arithmetic: 2.21 us -> none  [body(): grad_rows.astype(F32)]
where the time goes in v3:
time: 83.9 us; the launch traced here: 83.7 us
  Pallas kernels  83 us (99%)
    pallas_call x1, Pallas kernels, body(): pl.pallas_call(kernel, out_shape=(jax.ShapeDtypeStruct((1, TOK, CH), BF16...  80.2 us
    pallas_call x1, Pallas kernels, body(): pl.pallas_call(write_out, out_shape=(jax.ShapeDtypeStruct((1, TOK, CH), B...  2.86 us

profile of v3, /device:TPU:1, one launch (start us, length us, event | category | flops | bytes accessed | tf_op | source)
XLA Modules:
  0.0 83.7 jit_solution(147821685173953258)
XLA Ops:
  0.6 80.2 %shard_map.101 = (bf16[1,256,2048]{2,1,0:T(8,128)(2,1)}, bf16[1,256,2048]{2,1,0:T(8,128)(2,1)}, bf16[128,2048]{1,0:T(8,128)(2,1)}, f32[31,128]{1,0:T(8,128)}, f32[1,2048]{1,0:T(1,128)}) custom-call(bf16[1,256,2048]{2,1,0:T(8,128)(2,1)} %v_hbm.1, bf16[1,256,2048]{2,1,0:T(8,128)(2,1)} %g_hbm.1, bf16[1,256,2048]{2,1,0:T(8,128)(2,1)} %u_hbm.1, ...), custom_call_target="tpu_custom_call" | custom-call | tf_op jit(solution)/shard_map/pallas_call | solution.py:654
  80.8 2.9 %shard_map.102 = (bf16[1,256,2048]{2,1,0:T(8,128)(2,1)}, bf16[1,256,2048]{2,1,0:T(8,128)(2,1)}, f32[128,2048]{1,0:T(8,128)}, f32[31,128]{1,0:T(8,128)}, f32[1,2048]{1,0:T(1,128)}) custom-call(bf16[1,256,2048]{2,1,0:T(8,128)(2,1)} %get-tuple-element.15.gv, bf16[1,256,2048]{2,1,0:T(8,128)(2,1)} %get-tuple-element.16.gt, ...), custom_call_target="tpu_custom_call" | custom-call | tf_op jit(solution)/shard_map/pallas_call | solution.py:717

commit v4 on v3

--- a/solution.py
+++ b/solution.py
@@ -26,8 +26,9 @@
 
 
 def kernel(
-    v_hbm, g_hbm, u_hbm, w_hbm, taps_ref, gain_ref,
-    gv_hbm, gt_hbm, gw_ref, dt_ref, dn_ref,
+    v_hbm, g_hbm, u_hbm, w_hbm, taps_hbm, gain_hbm,
+    gv_hbm, gt_hbm, gw_hbm, dt_hbm, dn_hbm,
+    gain_ref, gw_ref, dt_ref, dn_ref,
     v_s, g_s, u_s, usib, wbuf, tapsb, glu, conv, act, actsib, ut,
     pbuf, r1, r2, q, s1, s2, vz, rz, fg, gacc, gpad, mean_s, inv_s, gate_a, gate_b, gv_s, gt_s,
     halo_out, halo_in, ghalo_out, ghalo_in, dn, tg, tr, tz, tsib, tfin, gfull, dr, dz, dfin, dsib,
@@ -64,9 +65,11 @@
         pltpu.make_async_copy(v_hbm.at[0], v_s, local_sem.at[1]),
         pltpu.make_async_copy(g_hbm.at[0], g_s, local_sem.at[2]),
         pltpu.make_async_copy(u_hbm.at[0], u_s, local_sem.at[3]),
+        pltpu.make_async_copy(taps_hbm, tapsb.at[sp, pl.ds(0, TAPS)], local_sem.at[12]),
+        pltpu.make_async_copy(gain_hbm, gain_ref, local_sem.at[13]),
     ]
-    for load in loads:
-        load.start()
+    for at in (1, 2, 4, 5, 0, 3):
+        loads[at].start()
 
     barrier = pltpu.get_barrier_semaphore()
     pl.semaphore_signal(barrier, inc=1, device_id=sibling, device_id_type=MESH)
@@ -75,7 +78,33 @@
     for d in range(1, 16):
         pl.semaphore_signal(barrier, inc=1, device_id=spdev(d), device_id_type=MESH)
 
-    tapsb[sp, :TAPS] = taps_ref[...]
+    for load in loads[1:3]:
+        load.wait()
+    def glu_rows(r):
+        rows = pl.ds(r, 32)
+        for c in range(NC):
+            lanes = slice(128 * c, 128 * c + 128)
+            value = v_s[rows, lanes].astype(F32)
+            sig = jax.nn.sigmoid(g_s[rows, lanes].astype(F32))
+            wide = value * sig
+            gate_a[c, rows, :] = sig
+            gate_b[c, rows, :] = wide * (1.0 - sig)
+            narrow = wide.astype(BF16)
+            glu[c, pl.ds(r + 32, 32), :] = narrow.astype(F32)
+            yield lanes, narrow
+
+    for lanes, narrow in glu_rows(TOK - 32):
+        halo_out[:, lanes] = narrow
+
+    def glu_step(i, carry):
+        for _ in glu_rows(pl.multiple_of(i * 32, 32)):
+            pass
+        return carry
+
+    lax.fori_loop(0, TOK // 32 - 1, glu_step, 0)
+
+    for load in loads[3:]:
+        load.wait()
     tapsb[sp, TAPS:] = jnp.zeros((1, 128), F32)
     loads[0].wait()
     pl.semaphore_wait(barrier, 23)
@@ -141,34 +170,9 @@
     }
     w_send(0, 1, 0)
     w_send(0, 1, 1)
-    for load in loads[1:]:
-        load.wait()
+    halo_copy = send(halo_out, halo_in, spdev(1))
     u_copy = send(u_s, usib, sibling)
     w_share(0)
-
-    def glu_rows(r):
-        rows = pl.ds(r, 32)
-        for c in range(NC):
-            lanes = slice(128 * c, 128 * c + 128)
-            value = v_s[rows, lanes].astype(F32)
-            sig = jax.nn.sigmoid(g_s[rows, lanes].astype(F32))
-            wide = value * sig
-            gate_a[c, rows, :] = sig
-            gate_b[c, rows, :] = wide * (1.0 - sig)
-            narrow = wide.astype(BF16)
-            glu[c, pl.ds(r + 32, 32), :] = narrow.astype(F32)
-            yield lanes, narrow
-
-    for lanes, narrow in glu_rows(TOK - 32):
-        halo_out[:, lanes] = narrow
-    halo_copy = send(halo_out, halo_in, spdev(1))
-
-    def glu_step(i, carry):
-        for _ in glu_rows(pl.multiple_of(i * 32, 32)):
-            pass
-        return carry
-
-    lax.fori_loop(0, TOK // 32 - 1, glu_step, 0)
 
     u_copy.wait_recv()
 
@@ -181,21 +185,30 @@
 
     lax.fori_loop(0, NZ, transpose_step, 0)
 
+    def correlate(taps, read):
+        sums = {}
+        for o in range(8 * 7 + TAPS):
+            x = read(o)
+            for k in range(8):
+                j = o - 8 * k
+                if 0 <= j < TAPS:
+                    term = taps[j] * x
+                    key = k, j % 2
+                    sums[key] = sums[key] + term if key in sums else term
+                    if j == TAPS - 1:
+                        yield k, sums.pop((k, 0)) + sums.pop((k, 1))
+
     mean_s[...] = jnp.zeros_like(mean_s)
 
     def conv_chunk(first, last, c, carry):
         taps = [jnp.broadcast_to(tapsb[c, j : j + 1, :], (8, 128)) for j in range(TAPS)]
 
         def rows_step(i, carry):
-            for k in range(8):
-                r = pl.multiple_of(i * 64, 64) + 8 * k
-                parts = [None] * 2
-                for j in range(TAPS):
-                    term = taps[j] * glu[c, pl.ds(r + 2 + j, 8), :]
-                    parts[j % 2] = term if parts[j % 2] is None else parts[j % 2] + term
-                total = (parts[0] + parts[1]).astype(BF16).astype(F32)
-                conv[c, pl.ds(r, 8), :] = total
-                mean_s[pl.ds(r, 8), :] += total
+            base = pl.multiple_of(i * 64, 64)
+            for k, total in correlate(taps, lambda o: glu[c, pl.ds(base + 2 + o, 8), :]):
+                total = total.astype(BF16).astype(F32)
+                conv[c, pl.ds(base + 8 * k, 8), :] = total
+                mean_s[pl.ds(base + 8 * k, 8), :] += total
             return carry
 
         return lax.fori_loop(first, last, rows_step, carry)
@@ -249,11 +262,6 @@
     w_event(2, 0)
     norm_part(2)
     norm_part(3)
-    w_share(1)
-    w_share(7)
-    for copy in act_copies:
-        copy.wait_recv()
-
     axes = ((("sp_1", cx), ("sp_0", cy)), (("sp_0", cy), ("sp_1", cx)))
 
     def near(axis, d):
@@ -392,42 +400,47 @@
 
         lax.fori_loop(0, 4, step, 0)
 
+    grad_block((0,), first=True)
+    w_event(2, 1)
+    w_share(1)
+    w_share(7)
+    for copy in act_copies:
+        copy.wait_recv()
     partial_sums(0)
     rs1_send(0)
-    w_event(2, 1)
     partial_sums(1)
     rs1_send(1)
     w_rest(2, 0)
     partial_sums(2)
     rs1_send(2)
-    w_event(3, 0)
     partial_sums(3)
     rs1_send(3)
-    grad_block((0, 1, 7), first=True)
+    w_event(3, 0)
+    w_rest(2, 1)
     rs1_mid(0)
-    w_rest(2, 1)
     w_event(3, 1)
-    rs1_mid(1)
     w_share(2)
     w_share(6)
+    rs1_mid(1)
+    grad_block((1, 7))
+    w_rest(3, 0)
     grad_block((2, 6))
-    w_rest(3, 0)
-    w_event(4, 0)
-    w_event(4, 1)
     w_rest(3, 1)
+    w_share(3)
+    w_share(5)
     rs1_fin(0)
     rs1_mid(2)
-    w_share(3)
-    w_share(5)
+    grad_block((3, 5))
     rs1_fin(1)
     rs1_mid(3)
     rs2_mid(0)
-    grad_block((3, 5))
+    w_event(4, 0)
+    w_event(4, 1)
     w_rest(4, 0)
     w_rest(4, 1)
     w_share(4)
+    rs1_fin(2)
     rs2_mid(1)
-    rs1_fin(2)
     grad_block((4,))
 
     dn[...] = jnp.zeros_like(dn)
@@ -501,17 +514,19 @@
     def taps_chunk(c, carry):
         def rows_step(i, sums):
             sums = list(sums)
-            for k in range(4):
-                r = pl.multiple_of(i * 32, 32) + 8 * k
-                g = gpad[c, pl.ds(r, 8), :]
-                for j in range(TAPS):
-                    sums[j] = sums[j] + g * glu[c, pl.ds(r + 2 + j, 8), :]
+            base = pl.multiple_of(i * 64, 64)
+            g = [gpad[c, pl.ds(base + 8 * k, 8), :] for k in range(8)]
+            for o in range(8 * 7 + TAPS):
+                x = glu[c, pl.ds(base + 2 + o, 8), :]
+                for k in range(8):
+                    j = o - 8 * k
+                    if 0 <= j < TAPS:
+                        sums[j] = sums[j] + g[k] * x
             return tuple(sums)
 
-        sums = lax.fori_loop(0, TOK // 32, rows_step, tuple(jnp.zeros((8, 128), F32) for _ in range(TAPS)))
-        for j in range(TAPS):
-            tg[c, j : j + 1, :] = jnp.sum(sums[j], axis=0, keepdims=True)
-        tg[c, TAPS:, :] = jnp.zeros((1, 128), F32)
+        sums = lax.fori_loop(0, TOK // 64, rows_step, tuple(jnp.zeros((8, 128), F32) for _ in range(TAPS)))
+        rows = [jnp.sum(total, axis=0, keepdims=True) for total in sums] + [jnp.zeros((1, 128), F32)]
+        tg[c] = jnp.concatenate(rows, axis=0).astype(BF16)
         return carry
 
     part_copies = []
@@ -527,20 +542,18 @@
                 )
 
     rs2_fin(0)
+    taps_group(2)
+    rs1_fin(3)
     rs2_mid(2)
-    rs1_fin(3)
-    taps_group(2)
+    taps_group(1)
     rs2_fin(1)
-    taps_group(1)
-    gain_z = gain_sum()
+    taps_group(3)
     rs2_mid(3)
     rs2_fin(2)
-    taps_group(3)
+    gain_z = gain_sum()
+    taps_group(0)
+    rs3(0)
     rs2_fin(3)
-    rs3(0)
-    taps_group(0)
-    gain_last = gain_pair(gain_z)
-    rs3(1)
 
     ghalo_copy.wait_recv()
     keep_g = (sp < 15).astype(F32)
@@ -548,25 +561,21 @@
         gpad[c, TOK:, :] = ghalo_in[:, 128 * c : 128 * c + 128].astype(F32) * keep_g
 
     def grad_chunk(c, carry):
-        taps = [jnp.broadcast_to(tapsb[c, j : j + 1, :], (8, 128)) for j in range(TAPS)]
+        taps = [jnp.broadcast_to(tapsb[c, j : j + 1, :], (8, 128)) for j in reversed(range(TAPS))]
         lanes = pl.ds(pl.multiple_of(c * 128, 128), 128)
 
         def rows_step(i, carry):
             base = pl.multiple_of(i * 64, 64)
-            for pair in range(4):
-                values, gates = [], []
-                for k in (2 * pair, 2 * pair + 1):
-                    r = base + 8 * k
-                    parts = [None] * 2
-                    for j in range(TAPS):
-                        term = taps[j] * gpad[c, pl.ds(r + 30 - j, 8), :]
-                        parts[j % 2] = term if parts[j % 2] is None else parts[j % 2] + term
-                    total = (parts[0] + parts[1]).astype(BF16).astype(F32)
-                    values.append(total * gate_a[c, pl.ds(r, 8), :])
-                    gates.append(total * gate_b[c, pl.ds(r, 8), :])
-                rows = pl.ds(base + 16 * pair, 16)
-                gv_s[rows, lanes] = jnp.concatenate(values, axis=0).astype(BF16)
-                gt_s[rows, lanes] = jnp.concatenate(gates, axis=0).astype(BF16)
+            values, gates = [], []
+            for k, total in correlate(taps, lambda o: gpad[c, pl.ds(base + o, 8), :]):
+                total = total.astype(BF16).astype(F32)
+                values.append(total * gate_a[c, pl.ds(base + 8 * k, 8), :])
+                gates.append(total * gate_b[c, pl.ds(base + 8 * k, 8), :])
+                if k % 2:
+                    rows = pl.ds(base + 8 * k - 8, 16)
+                    gv_s[rows, lanes] = jnp.concatenate(values, axis=0).astype(BF16)
+                    gt_s[rows, lanes] = jnp.concatenate(gates, axis=0).astype(BF16)
+                    values, gates = [], []
             return carry
 
         return lax.fori_loop(0, TOK // 64, rows_step, carry)
@@ -584,18 +593,20 @@
             stores.append(copy)
 
     grad_group(0)
-    gain_copies2 = gain_out(gain_last)
+    rs3(1)
+    grad_group(1)
     rs3(2)
-    grad_group(1)
-    total = tg[sp]
+    gain_last = gain_pair(gain_z)
+    total = tg[sp].astype(F32)
     for copy in part_copies:
         copy.wait_recv()
     for d in range(1, 16):
-        total = total + tr[d]
+        total = total + tr[d].astype(F32)
     tz[cz] = total
     tz_copies = [send(tz.at[cz], tz.at[cz], zdev(d)) for d in range(1, NZ)]
     rs3(3)
     grad_group(2)
+    gain_copies2 = gain_out(gain_last)
     grad_group(3)
 
     for copy in tz_copies:
@@ -615,12 +626,20 @@
             gw_ref[16 * x : 16 * x + 16, lane : lane + 128] = fg[t, s, 0]
             lane = 512 * t + 128 * x
             gw_ref[64 + 16 * y : 80 + 16 * y, lane : lane + 128] = fg[t, s, 1]
+    def store(held, target):
+        copy = pltpu.make_async_copy(held, target, local_sem.at[14 + len(stores) - 8])
+        copy.start()
+        stores.append(copy)
+
+    store(gw_ref, gw_hbm)
     for copy in gain_copies2:
         copy.wait_recv()
     for c in range(NC):
         dn_ref[:, 128 * c : 128 * c + 128] = jnp.sum(gfull[c], axis=0, keepdims=True)
+    store(dn_ref, dn_hbm)
     pair_copy.wait_recv()
     dt_ref[...] = (tfin[...] + tsib[...])[:TAPS]
+    store(dt_ref, dt_hbm)
     for copy in stores:
         copy.wait()
     for copy in started:
@@ -649,7 +668,6 @@
 
 
 def body(value_half, gate_half, upstream, conv_taps, norm_gain, out_weight):
-    vmem = pl.BlockSpec(memory_space=pltpu.VMEM)
     hbm = pl.BlockSpec(memory_space=pl.ANY)
     grad_value, grad_gate, grad_rows, taps, gain = pl.pallas_call(
         kernel,
@@ -660,9 +678,13 @@
             jax.ShapeDtypeStruct((TAPS, 128), F32),
             jax.ShapeDtypeStruct((1, CH), F32),
         ),
-        in_specs=[hbm] * 4 + [vmem] * 2,
-        out_specs=[hbm] * 2 + [vmem] * 3,
+        in_specs=[hbm] * 6,
+        out_specs=[hbm] * 5,
         scratch_shapes=[
+            pltpu.VMEM((1, CH), F32),
+            pltpu.VMEM((128, CH), BF16),
+            pltpu.VMEM((TAPS, 128), F32),
+            pltpu.VMEM((1, CH), F32),
             pltpu.VMEM((TOK, CH), BF16),
             pltpu.VMEM((TOK, CH), BF16),
             pltpu.VMEM((TOK, CH), BF16),
@@ -696,8 +718,8 @@
             pltpu.VMEM((32, CH), BF16),
             pltpu.VMEM((32, CH), BF16),
             pltpu.VMEM((NC, 8, 128), F32),
-            pltpu.VMEM((NC, 32, 128), F32),
-            pltpu.VMEM((16, 32, 128), F32),
+            pltpu.VMEM((NC, 32, 128), BF16),
+            pltpu.VMEM((16, 32, 128), BF16),
             pltpu.VMEM((NZ, 32, 128), F32),
             pltpu.VMEM((32, 128), F32),
             pltpu.VMEM((32, 128), F32),
@@ -706,7 +728,7 @@
             pltpu.VMEM((NZ, 8, 128), F32),
             pltpu.VMEM((8, 128), F32),
             pltpu.VMEM((8, 128), F32),
-            pltpu.SemaphoreType.DMA((12,)),
+            pltpu.SemaphoreType.DMA((17,)),
             pltpu.SemaphoreType.DMA((N_SEND,)),
             pltpu.SemaphoreType.DMA((N_SEND,)),
         ],

time: 83.9 us -> 78.3 us (0.933)
  Pallas kernels: 83 us -> 77.5 us
    pallas_call x1, Pallas kernels: 80.2 us -> 74.7 us  [body(): pl.pallas_call(kernel, out_shape=(jax.ShapeDtypeStruct((1, TOK, CH), BF16...]
where the time goes in v4:
time: 78.3 us; the launch traced here: 78.2 us
  Pallas kernels  77.5 us (99%)
    pallas_call x1, Pallas kernels, body(): pl.pallas_call(kernel, out_shape=(jax.ShapeDtypeStruct((1, TOK, CH), BF16...  74.7 us
    pallas_call x1, Pallas kernels, body(): pl.pallas_call(write_out, out_shape=(jax.ShapeDtypeStruct((1, TOK, CH), B...  2.86 us

profile of v4, /device:TPU:1, one launch (start us, length us, event | category | flops | bytes accessed | tf_op | source)
XLA Modules:
  0.0 78.2 jit_solution(9880105025928626501)
XLA Ops:
  0.6 74.7 %shard_map.101 = (bf16[1,256,2048]{2,1,0:T(8,128)(2,1)}, bf16[1,256,2048]{2,1,0:T(8,128)(2,1)}, bf16[128,2048]{1,0:T(8,128)(2,1)}, f32[31,128]{1,0:T(8,128)}, f32[1,2048]{1,0:T(1,128)}) custom-call(bf16[1,256,2048]{2,1,0:T(8,128)(2,1)} %v_hbm.1, bf16[1,256,2048]{2,1,0:T(8,128)(2,1)} %g_hbm.1, bf16[1,256,2048]{2,1,0:T(8,128)(2,1)} %u_hbm.1, ...), custom_call_target="tpu_custom_call" | custom-call | tf_op jit(solution)/shard_map/pallas_call | solution.py:672
  75.3 2.9 %shard_map.102 = (bf16[1,256,2048]{2,1,0:T(8,128)(2,1)}, bf16[1,256,2048]{2,1,0:T(8,128)(2,1)}, f32[128,2048]{1,0:T(8,128)}, f32[31,128]{1,0:T(8,128)}, f32[1,2048]{1,0:T(1,128)}) custom-call(bf16[1,256,2048]{2,1,0:T(8,128)(2,1)} %get-tuple-element.15.gv, bf16[1,256,2048]{2,1,0:T(8,128)(2,1)} %get-tuple-element.16.gt, ...), custom_call_target="tpu_custom_call" | custom-call | tf_op jit(solution)/shard_map/pallas_call | solution.py:739

commit v5 on v4

--- a/solution.py
+++ b/solution.py
@@ -130,10 +130,14 @@
                 wbuf.at[src, cc, rows, lanes[way]], wbuf.at[dst, cc, rows, lanes[way]], zdev(sign)
             )
 
-    def w_share(rel):
-        for turn in range(4):
-            arrived(w_quarters, (rel, turn))
-        w_pair[rel] = send(wbuf.at[rel, cc], wbuf.at[rel, cc], sibling)
+    def w_share(rels, half, sub):
+        at = parity if half == 0 else 1 - parity
+        rows = pl.ds(pl.multiple_of(64 * at + 32 * sub, 32), 32)
+        for rel in rels:
+            w_pair.setdefault(rel, []).append(send(wbuf.at[rel, cc, rows], wbuf.at[rel, cc, rows], sibling))
+
+    def blocks_at(step):
+        return sorted({step, NZ - step})
 
     def w_event(step, sub):
         for way in (0, 1):
@@ -148,17 +152,19 @@
                     w_quarters[rel, turn] = send(
                         wbuf.at[rel, cc, rows], wbuf.at[rel, cc, rows], {name: lax.rem(at + sign + 4, 4)}
                     )
+        w_share(blocks_at(step), 0, sub)
 
     def w_rest(step, sub):
-        if step == 2:
-            for rel in (2, 6):
+        if step < 3:
+            for rel in blocks_at(step):
                 for turn in (2 * sub, 2 * sub + 1):
                     arrived(w_quarters, (rel, turn))
         else:
             for way in (0, 1):
                 arrived(w_copies, (1, step, sub, way))
-        if step < 4:
+        if step in (2, 3):
             w_send(1, step + 1, sub)
+        w_share(blocks_at(step), 1, sub)
 
     taps_copies = {
         dy: [
@@ -172,7 +178,7 @@
     w_send(0, 1, 1)
     halo_copy = send(halo_out, halo_in, spdev(1))
     u_copy = send(u_s, usib, sibling)
-    w_share(0)
+    w_pair[0] = [send(wbuf.at[0, cc], wbuf.at[0, cc], sibling)]
 
     u_copy.wait_recv()
 
@@ -379,7 +385,8 @@
 
     def grad_block(rels, first=False):
         for rel in rels:
-            w_pair[rel].wait_recv()
+            for copy in w_pair[rel]:
+                copy.wait_recv()
         lhs = []
         for rel in rels:
             zb = lax.rem(cz + rel, NZ)
@@ -402,8 +409,8 @@
 
     grad_block((0,), first=True)
     w_event(2, 1)
-    w_share(1)
-    w_share(7)
+    w_rest(1, 0)
+    w_rest(1, 1)
     for copy in act_copies:
         copy.wait_recv()
     partial_sums(0)
@@ -419,29 +426,24 @@
     w_rest(2, 1)
     rs1_mid(0)
     w_event(3, 1)
-    w_share(2)
-    w_share(6)
     rs1_mid(1)
     grad_block((1, 7))
     w_rest(3, 0)
     grad_block((2, 6))
+    w_event(4, 0)
     w_rest(3, 1)
-    w_share(3)
-    w_share(5)
     rs1_fin(0)
     rs1_mid(2)
+    w_event(4, 1)
     grad_block((3, 5))
+    w_rest(4, 0)
+    w_rest(4, 1)
     rs1_fin(1)
     rs1_mid(3)
     rs2_mid(0)
-    w_event(4, 0)
-    w_event(4, 1)
-    w_rest(4, 0)
-    w_rest(4, 1)
-    w_share(4)
+    grad_block((4,))
     rs1_fin(2)
     rs2_mid(1)
-    grad_block((4,))
 
     dn[...] = jnp.zeros_like(dn)
 
@@ -475,7 +477,6 @@
 
     for lanes, narrow in back_rows(0):
         ghalo_out[:, lanes] = narrow
-    ghalo_copy = send(ghalo_out, ghalo_in, spdev(-1))
 
     def back_step(i, carry):
         for _ in back_rows(pl.multiple_of(i * 32, 32)):
@@ -542,15 +543,16 @@
                 )
 
     rs2_fin(0)
+    rs1_fin(3)
+    ghalo_copy = send(ghalo_out, ghalo_in, spdev(-1))
     taps_group(2)
-    rs1_fin(3)
     rs2_mid(2)
+    rs2_fin(1)
     taps_group(1)
-    rs2_fin(1)
+    rs2_mid(3)
+    gain_z = gain_sum()
     taps_group(3)
-    rs2_mid(3)
     rs2_fin(2)
-    gain_z = gain_sum()
     taps_group(0)
     rs3(0)
     rs2_fin(3)
@@ -592,9 +594,8 @@
             copy.start()
             stores.append(copy)
 
+    rs3(1)
     grad_group(0)
-    rs3(1)
-    grad_group(1)
     rs3(2)
     gain_last = gain_pair(gain_z)
     total = tg[sp].astype(F32)
@@ -604,10 +605,13 @@
         total = total + tr[d].astype(F32)
     tz[cz] = total
     tz_copies = [send(tz.at[cz], tz.at[cz], zdev(d)) for d in range(1, NZ)]
+    grad_group(1)
     rs3(3)
     grad_group(2)
     gain_copies2 = gain_out(gain_last)
     grad_group(3)
+    for copy in started[:200]:
+        copy.wait_send()
 
     for copy in tz_copies:
         copy.wait_recv()
@@ -642,7 +646,7 @@
     store(dt_ref, dt_hbm)
     for copy in stores:
         copy.wait()
-    for copy in started:
+    for copy in started[200:]:
         copy.wait_send()
 
 

time: 78.3 us -> 77 us (0.983)
  Pallas kernels: 77.5 us -> 75.8 us
    pallas_call x1, Pallas kernels: 74.7 us -> 73 us  [body(): pl.pallas_call(kernel, out_shape=(jax.ShapeDtypeStruct((1, TOK, CH), BF16...]
where the time goes in v5:
time: 77 us; the launch traced here: 76.5 us
  Pallas kernels  75.8 us (98%)
    pallas_call x1, Pallas kernels, body(): pl.pallas_call(kernel, out_shape=(jax.ShapeDtypeStruct((1, TOK, CH), BF16...  73 us
    pallas_call x1, Pallas kernels, body(): pl.pallas_call(write_out, out_shape=(jax.ShapeDtypeStruct((1, TOK, CH), B...  2.86 us

profile of v5, /device:TPU:1, one launch (start us, length us, event | category | flops | bytes accessed | tf_op | source)
XLA Modules:
  0.0 76.5 jit_solution(16290107913447756635)
XLA Ops:
  0.6 73.0 %shard_map.101 = (bf16[1,256,2048]{2,1,0:T(8,128)(2,1)}, bf16[1,256,2048]{2,1,0:T(8,128)(2,1)}, bf16[128,2048]{1,0:T(8,128)(2,1)}, f32[31,128]{1,0:T(8,128)}, f32[1,2048]{1,0:T(1,128)}) custom-call(bf16[1,256,2048]{2,1,0:T(8,128)(2,1)} %v_hbm.1, bf16[1,256,2048]{2,1,0:T(8,128)(2,1)} %g_hbm.1, bf16[1,256,2048]{2,1,0:T(8,128)(2,1)} %u_hbm.1, ...), custom_call_target="tpu_custom_call" | custom-call | tf_op jit(solution)/shard_map/pallas_call | solution.py:676
  73.6 2.9 %shard_map.102 = (bf16[1,256,2048]{2,1,0:T(8,128)(2,1)}, bf16[1,256,2048]{2,1,0:T(8,128)(2,1)}, f32[128,2048]{1,0:T(8,128)}, f32[31,128]{1,0:T(8,128)}, f32[1,2048]{1,0:T(1,128)}) custom-call(bf16[1,256,2048]{2,1,0:T(8,128)(2,1)} %get-tuple-element.15.gv, bf16[1,256,2048]{2,1,0:T(8,128)(2,1)} %get-tuple-element.16.gt, ...), custom_call_target="tpu_custom_call" | custom-call | tf_op jit(solution)/shard_map/pallas_call | solution.py:743

commit v6 on v5

--- a/solution.py
+++ b/solution.py
@@ -65,8 +65,8 @@
         pltpu.make_async_copy(v_hbm.at[0], v_s, local_sem.at[1]),
         pltpu.make_async_copy(g_hbm.at[0], g_s, local_sem.at[2]),
         pltpu.make_async_copy(u_hbm.at[0], u_s, local_sem.at[3]),
-        pltpu.make_async_copy(taps_hbm, tapsb.at[sp, pl.ds(0, TAPS)], local_sem.at[12]),
-        pltpu.make_async_copy(gain_hbm, gain_ref, local_sem.at[13]),
+        pltpu.make_async_copy(taps_hbm, tapsb.at[sp, pl.ds(0, TAPS)], local_sem.at[4]),
+        pltpu.make_async_copy(gain_hbm, gain_ref, local_sem.at[5]),
     ]
     for at in (1, 2, 4, 5, 0, 3):
         loads[at].start()
@@ -442,8 +442,6 @@
     rs1_mid(3)
     rs2_mid(0)
     grad_block((4,))
-    rs1_fin(2)
-    rs2_mid(1)
 
     dn[...] = jnp.zeros_like(dn)
 
@@ -542,27 +540,24 @@
                     send(tg.at[4 * row + x], tr.at[4 * dy + dx], {"sp_0": row, "sp_1": x})
                 )
 
+    rs1_fin(2)
+    rs2_mid(1)
+    rs1_fin(3)
+    taps_group(2)
     rs2_fin(0)
-    rs1_fin(3)
+    rs2_mid(2)
+    taps_group(1)
+    rs2_fin(1)
+    rs2_mid(3)
     ghalo_copy = send(ghalo_out, ghalo_in, spdev(-1))
-    taps_group(2)
-    rs2_mid(2)
-    rs2_fin(1)
-    taps_group(1)
-    rs2_mid(3)
     gain_z = gain_sum()
     taps_group(3)
     rs2_fin(2)
     taps_group(0)
+    rs2_fin(3)
     rs3(0)
-    rs2_fin(3)
-
-    ghalo_copy.wait_recv()
-    keep_g = (sp < 15).astype(F32)
-    for c in range(NC):
-        gpad[c, TOK:, :] = ghalo_in[:, 128 * c : 128 * c + 128].astype(F32) * keep_g
-
-    def grad_chunk(c, carry):
+
+    def grad_chunk(first, last, c, carry):
         taps = [jnp.broadcast_to(tapsb[c, j : j + 1, :], (8, 128)) for j in reversed(range(TAPS))]
         lanes = pl.ds(pl.multiple_of(c * 128, 128), 128)
 
@@ -580,24 +575,35 @@
                     values, gates = [], []
             return carry
 
-        return lax.fori_loop(0, TOK // 64, rows_step, carry)
+        return lax.fori_loop(first, last, rows_step, carry)
 
     stores = []
 
+    def store(held, target):
+        copy = pltpu.make_async_copy(held, target, local_sem.at[6 + len(stores)])
+        copy.start()
+        stores.append(copy)
+
     def grad_group(at):
-        lax.fori_loop(4 * at, 4 * at + 4, grad_chunk, 0)
-        lanes = pl.ds(512 * at, 512)
-        for narrow, wide in ((gv_s, gv_hbm), (gt_s, gt_hbm)):
-            copy = pltpu.make_async_copy(
-                narrow.at[:, lanes], wide.at[0, :, lanes], local_sem.at[4 + len(stores)]
-            )
-            copy.start()
-            stores.append(copy)
+        lax.fori_loop(4 * at, 4 * at + 4, functools.partial(grad_chunk, 0, TOK // 64 - 1), 0)
+        rows, lanes = pl.ds(0, TOK - 64), pl.ds(512 * at, 512)
+        store(gv_s.at[rows, lanes], gv_hbm.at[0, rows, lanes])
+        store(gt_s.at[rows, lanes], gt_hbm.at[0, rows, lanes])
+
+    def grad_last():
+        ghalo_copy.wait_recv()
+        keep_g = (sp < 15).astype(F32)
+        for c in range(NC):
+            gpad[c, TOK:, :] = ghalo_in[:, 128 * c : 128 * c + 128].astype(F32) * keep_g
+        lax.fori_loop(0, NC, functools.partial(grad_chunk, TOK // 64 - 1, TOK // 64), 0)
+        rows = pl.ds(TOK - 64, 64)
+        store(gv_s.at[rows], gv_hbm.at[0, rows])
+        store(gt_s.at[rows], gt_hbm.at[0, rows])
 
     rs3(1)
     grad_group(0)
+    gain_last = gain_pair(gain_z)
     rs3(2)
-    gain_last = gain_pair(gain_z)
     total = tg[sp].astype(F32)
     for copy in part_copies:
         copy.wait_recv()
@@ -607,9 +613,10 @@
     tz_copies = [send(tz.at[cz], tz.at[cz], zdev(d)) for d in range(1, NZ)]
     grad_group(1)
     rs3(3)
+    gain_copies2 = gain_out(gain_last)
     grad_group(2)
-    gain_copies2 = gain_out(gain_last)
     grad_group(3)
+    grad_last()
     for copy in started[:200]:
         copy.wait_send()
 
@@ -630,11 +637,6 @@
             gw_ref[16 * x : 16 * x + 16, lane : lane + 128] = fg[t, s, 0]
             lane = 512 * t + 128 * x
             gw_ref[64 + 16 * y : 80 + 16 * y, lane : lane + 128] = fg[t, s, 1]
-    def store(held, target):
-        copy = pltpu.make_async_copy(held, target, local_sem.at[14 + len(stores) - 8])
-        copy.start()
-        stores.append(copy)
-
     store(gw_ref, gw_hbm)
     for copy in gain_copies2:
         copy.wait_recv()
@@ -732,7 +734,7 @@
             pltpu.VMEM((NZ, 8, 128), F32),
             pltpu.VMEM((8, 128), F32),
             pltpu.VMEM((8, 128), F32),
-            pltpu.SemaphoreType.DMA((17,)),
+            pltpu.SemaphoreType.DMA((19,)),
             pltpu.SemaphoreType.DMA((N_SEND,)),
             pltpu.SemaphoreType.DMA((N_SEND,)),
         ],

time: 77 us -> 75.5 us (0.981)
  Pallas kernels: 75.8 us -> 74.5 us
    pallas_call x1, Pallas kernels: 73 us -> 71.6 us  [body(): pl.pallas_call(kernel, out_shape=(jax.ShapeDtypeStruct((1, TOK, CH), BF16...]
where the time goes in v6:
time: 75.5 us; the launch traced here: 75.1 us
  Pallas kernels  74.5 us (99%)
    pallas_call x1, Pallas kernels, body(): pl.pallas_call(kernel, out_shape=(jax.ShapeDtypeStruct((1, TOK, CH), BF16...  71.6 us
    pallas_call x1, Pallas kernels, body(): pl.pallas_call(write_out, out_shape=(jax.ShapeDtypeStruct((1, TOK, CH), B...  2.86 us

profile of v6, /device:TPU:1, one launch (start us, length us, event | category | flops | bytes accessed | tf_op | source)
XLA Modules:
  0.0 75.1 jit_solution(16234372783772403205)
XLA Ops:
  0.6 71.6 %shard_map.101 = (bf16[1,256,2048]{2,1,0:T(8,128)(2,1)}, bf16[1,256,2048]{2,1,0:T(8,128)(2,1)}, bf16[128,2048]{1,0:T(8,128)(2,1)}, f32[31,128]{1,0:T(8,128)}, f32[1,2048]{1,0:T(1,128)}) custom-call(bf16[1,256,2048]{2,1,0:T(8,128)(2,1)} %v_hbm.1, bf16[1,256,2048]{2,1,0:T(8,128)(2,1)} %g_hbm.1, bf16[1,256,2048]{2,1,0:T(8,128)(2,1)} %u_hbm.1, ...), custom_call_target="tpu_custom_call" | custom-call | tf_op jit(solution)/shard_map/pallas_call | solution.py:678
  72.2 2.9 %shard_map.102 = (bf16[1,256,2048]{2,1,0:T(8,128)(2,1)}, bf16[1,256,2048]{2,1,0:T(8,128)(2,1)}, f32[128,2048]{1,0:T(8,128)}, f32[31,128]{1,0:T(8,128)}, f32[1,2048]{1,0:T(1,128)}) custom-call(bf16[1,256,2048]{2,1,0:T(8,128)(2,1)} %get-tuple-element.15.gv, bf16[1,256,2048]{2,1,0:T(8,128)(2,1)} %get-tuple-element.16.gt, ...), custom_call_target="tpu_custom_call" | custom-call | tf_op jit(solution)/shard_map/pallas_call | solution.py:745

commit v7 on v6

--- a/solution.py
+++ b/solution.py
@@ -655,7 +655,13 @@
 def write_out(gv, gt, gw, dt, dn, gv_out, gt_out, gw_out, dt_out, dn_out, gv_s, gt_s, gw_s, gw_wide, dt_s, dn_s, sem):
     copies = []
     for i, (source, held, target) in enumerate(
-        ((gw, gw_s, gw_out), (gv, gv_s, gv_out), (gt, gt_s, gt_out), (dt, dt_s, dt_out), (dn, dn_s, dn_out))
+        [(gw, gw_s, gw_out)]
+        + [
+            tuple(ref.at[:, pl.ds(128 * half, 128)] for ref in refs)
+            for refs in ((gv, gv_s, gv_out), (gt, gt_s, gt_out))
+            for half in range(2)
+        ]
+        + [(dt, dt_s, dt_out), (dn, dn_s, dn_out)]
     ):
         copy = pltpu.make_async_copy(source, held, sem.at[0, i])
         copy.start()
@@ -760,7 +766,7 @@
             pltpu.VMEM((128, CH), F32),
             pltpu.VMEM((TAPS, 128), F32),
             pltpu.VMEM((1, CH), F32),
-            pltpu.SemaphoreType.DMA((2, 5)),
+            pltpu.SemaphoreType.DMA((2, 7)),
         ],
         compiler_params=pltpu.CompilerParams(vmem_limit_bytes=60_000_000),
     )(grad_value, grad_gate, grad_rows, taps, gain)

time: 75.5 us -> 75.5 us (level)
  no operation moved by 1% of the time
where the time goes in v7:
time: 75.5 us; the launch traced here: 75.1 us
  Pallas kernels  74.5 us (99%)
    pallas_call x1, Pallas kernels, body(): pl.pallas_call(kernel, out_shape=(jax.ShapeDtypeStruct((1, TOK, CH), BF16...  71.6 us
    pallas_call x1, Pallas kernels, body(): pl.pallas_call(write_out, out_shape=(jax.ShapeDtypeStruct((1, TOK, CH), B...  2.89 us

profile of v7, /device:TPU:1, one launch (start us, length us, event | category | flops | bytes accessed | tf_op | source)
XLA Modules:
  0.0 75.1 jit_solution(13800234153782411416)
XLA Ops:
  0.6 71.6 %shard_map.101 = (bf16[1,256,2048]{2,1,0:T(8,128)(2,1)}, bf16[1,256,2048]{2,1,0:T(8,128)(2,1)}, bf16[128,2048]{1,0:T(8,128)(2,1)}, f32[31,128]{1,0:T(8,128)}, f32[1,2048]{1,0:T(1,128)}) custom-call(bf16[1,256,2048]{2,1,0:T(8,128)(2,1)} %v_hbm.1, bf16[1,256,2048]{2,1,0:T(8,128)(2,1)} %g_hbm.1, bf16[1,256,2048]{2,1,0:T(8,128)(2,1)} %u_hbm.1, ...), custom_call_target="tpu_custom_call" | custom-call | tf_op jit(solution)/shard_map/pallas_call | solution.py:684
  72.2 2.9 %shard_map.102 = (bf16[1,256,2048]{2,1,0:T(8,128)(2,1)}, bf16[1,256,2048]{2,1,0:T(8,128)(2,1)}, f32[128,2048]{1,0:T(8,128)}, f32[31,128]{1,0:T(8,128)}, f32[1,2048]{1,0:T(1,128)}) custom-call(bf16[1,256,2048]{2,1,0:T(8,128)(2,1)} %get-tuple-element.15.gv, bf16[1,256,2048]{2,1,0:T(8,128)(2,1)} %get-tuple-element.16.gt, ...), custom_call_target="tpu_custom_call" | custom-call | tf_op jit(solution)/shard_map/pallas_call | solution.py:751
